TPU v7x, 32 devices: a whole 2x2x4 slice. The times are simulated.
32 devices in a mesh: rep: 2 (over x), fs: 8 (over z, y), tp: 2 (over core).
Axes of the slice: x: 2, y: 2, z: 4, core: 2. Of those that a mesh axis runs over, the one named last changes fastest.
Arguments:
- tokens: bfloat16 [6144, 2048], P(('rep', 'fs', 'tp')), may hold values from -6 to 6
- mix_gain_in: float32 [2048], replicated, may hold values from 0.1 to 1.9
- pool_weight: bfloat16 [4, 512, 512], P(None, 'fs'), may hold values from -0.25 to 0.25
- mix_gain_out: float32 [2048], replicated, may hold values from 0.1 to 1.9
- ffn_gain_in: float32 [2048], replicated, may hold values from 0.1 to 1.9
- gate_weight: bfloat16 [2048, 5632], P('fs', 'tp'), may hold values from -0.125 to 0.125
- up_weight: bfloat16 [2048, 5632], P('fs', 'tp'), may hold values from -0.125 to 0.125
- gate_taps: float32 [3, 5632], replicated, may hold values from -3.5 to 3.5
- up_taps: float32 [3, 5632], replicated, may hold values from -3.5 to 3.5
- down_weight: bfloat16 [5632, 2048], P('tp', 'fs'), may hold values from -0.078125 to 0.078125
- ffn_gain_out: float32 [2048], replicated, may hold values from 0.1 to 1.9
Outputs:
- mixed_out: bfloat16 [6144, 2048], P(('rep', 'fs', 'tp'))
All inputs are finite; a program needn't handle non-finite values.
Results may differ from a plain program's by a relative error of at most 0.014.
Values may be sent and summed in bfloat16 or wider, within the bound.
A program may use at most 128 MiB of HBM per device.

v0:
```python
import functools

import jax
import jax.numpy as jnp
from jax import lax
from jax.experimental import pallas as pl
from jax.experimental.pallas import tpu as pltpu
from jax.sharding import PartitionSpec as P

MESH = pl.DeviceIdType.MESH
pool_spans = (2, 4, 8, 16)
rms_eps = 1e-06
weight_budget = 24 * 2**20
f32 = jnp.float32
bf16 = jnp.bfloat16


def rms_scale(floats, gain):
    return floats * lax.rsqrt(jnp.mean(floats * floats, axis=-1, keepdims=True) + rms_eps) * gain


def gelu(v):
    return 0.5 * v * (1.0 + jnp.tanh(0.7978845608028654 * (v + 0.044715 * v * v * v)))


class Plan:
    def __init__(self, mesh, depth, width, columns):
        self.R, self.F, self.T = mesh.shape["rep"], mesh.shape["fs"], mesh.shape["tp"]
        self.Y = 1
        while 4 * self.Y * self.Y <= self.F:
            self.Y *= 2
        while self.F % self.Y:
            self.Y -= 1
        self.Z = self.F // self.Y
        self.joined = 3 * width * columns * 2 > weight_budget
        self.n_sub = self.R * self.Y if self.joined else 1
        self.G = self.T * self.n_sub
        self.cols = columns // self.n_sub


def kernel(
    plan, tokens, gain_in, pool, gain_out, gain_ffn, gate_t, up_t, down_w, gate_taps, up_taps, gain_last, out,
    halo, pool_all, w_gu, w_d, x_all, normed, after, acc_g, acc_u, hidden, partial, swapped, summed, got,
    own_sem, halo_sem, y_ss, up_ss, dn_ss, piece_rs, share_ss, share_rs, x_ss, x_rs, f_ss, s_ss, s_rs, p_ss, p_rs,
):
    R, F, T, Y, Z, G, cols = plan.R, plan.F, plan.T, plan.Y, plan.Z, plan.G, plan.cols
    r, f, t = lax.axis_index("rep"), lax.axis_index("fs"), lax.axis_index("tp")
    z, y = f // Y, f % Y
    rows, width = tokens.shape
    depth = width // F
    groups, gc = pool_all.shape[0], pool_all.shape[1]
    slab = gc // F
    S = min(T, groups)
    GS = groups // S
    q = t % S
    margin = halo.shape[0]
    C = G // T
    POOL, GA, UP, DN = 0, 1, 2, 3
    kinds = (POOL, GA, UP, DN)
    GU = (GA, UP)

    chip = r * Y + y if plan.joined else 0
    me = chip * T + t

    def peer(step):
        to = (chip + step) % C
        return {"rep": to // Y, "fs": z * Y + to % Y}

    def sub_of(y_to):
        return r * Y + y_to if plan.joined else 0

    def w_rows(y_to):
        return pl.ds(pl.multiple_of(sub_of(y_to) * cols, 64 if cols % 64 == 0 else 8), cols)

    def slot(kind, origin):
        if kind == POOL:
            return pool_all.at[pl.ds(q * GS, GS), pl.ds(pl.multiple_of(origin * slab, slab), slab)]
        return w_d.at[origin] if kind == DN else w_gu.at[origin, kind - GA]

    def source(kind, y_to):
        if kind == POOL:
            return pool.at[pl.ds(q * GS, GS)]
        return (gate_t, up_t, down_w)[kind - GA].at[w_rows(y_to)]

    def own_copy(kind):
        return pltpu.make_async_copy(source(kind, y), slot(kind, f), own_sem.at[kind])

    def y_copy(kind, step):
        y_to = (y + step) % Y
        return pltpu.make_async_remote_copy(
            src_ref=source(kind, y_to), dst_ref=slot(kind, f), send_sem=y_ss.at[kind, step - 1],
            recv_sem=piece_rs.at[kind, f], device_id={"fs": z * Y + y_to}, device_id_type=MESH)

    def chain_copy(kind, origin, dz):
        return pltpu.make_async_remote_copy(
            src_ref=slot(kind, origin), dst_ref=slot(kind, origin), send_sem=(up_ss if dz > 0 else dn_ss).at[kind, origin],
            recv_sem=piece_rs.at[kind, origin], device_id={"fs": (z + dz) * Y + y}, device_id_type=MESH)

    def arrived(kind, origin):
        chain_copy(kind, origin, 1).wait_recv()

    def pass_on(kind, origin, z0):
        @pl.when((z0 <= z) & (z + 1 < Z))
        def _():
            chain_copy(kind, origin, 1).start()

        @pl.when((z0 >= z) & (z > 0))
        def _():
            chain_copy(kind, origin, -1).start()

    side = jnp.minimum(z, Z - 1 - z)

    def place(k):
        j = k // Y
        near = jnp.where(j % 2 == 1, z - (j + 1) // 2, z + j // 2)
        far = jnp.where(2 * z <= Z - 1, j, Z - 1 - j)
        z0 = jnp.where(j <= 2 * side, near, far)
        return z0, z0 * Y + (y + k % Y) % Y

    def chain(kinds_now, k):
        z0, origin = place(k)
        for kind in kinds_now:
            arrived(kind, origin)
            pass_on(kind, origin, z0)

    def chain_own(kinds_now):
        for kind in kinds_now:
            own_copy(kind).wait()
            pass_on(kind, f, z)

    def chain_range(kinds_now, first, last):
        def body(k, carry):
            chain(kinds_now, k)
            return carry
        lax.fori_loop(first, last, body, 0)

    def halo_copy():
        return pltpu.make_async_remote_copy(
            src_ref=tokens.at[pl.ds(rows - margin, margin)], dst_ref=halo, send_sem=halo_sem.at[0],
            recv_sem=halo_sem.at[1], device_id={"tp": (t + 1) % T}, device_id_type=MESH)

    def share_copy(step, q_from):
        return pltpu.make_async_remote_copy(
            src_ref=pool_all.at[pl.ds(q_from * GS, GS)], dst_ref=pool_all.at[pl.ds(q_from * GS, GS)],
            send_sem=share_ss.at[step - 1], recv_sem=share_rs.at[q_from],
            device_id={"tp": t - q + (q + step) % S}, device_id_type=MESH)

    def x_copy(step, c_from):
        g = c_from * T + t
        return pltpu.make_async_remote_copy(
            src_ref=x_all.at[g], dst_ref=x_all.at[g], send_sem=x_ss.at[step - 1],
            recv_sem=x_rs.at[g], device_id=peer(step), device_id_type=MESH)

    def x_across(step, c, t_from):
        g = c * T + t_from
        return pltpu.make_async_remote_copy(
            src_ref=x_all.at[g], dst_ref=x_all.at[g], send_sem=f_ss.at[step - 1, c],
            recv_sem=x_rs.at[g], device_id={"tp": (t + step) % T}, device_id_type=MESH)

    def s_copy(step, block, t_from):
        t_to = (t + step) % T
        return pltpu.make_async_remote_copy(
            src_ref=partial.at[block, t_to], dst_ref=swapped.at[block, t_from], send_sem=s_ss.at[block, step - 1],
            recv_sem=s_rs.at[block, t_from], device_id={"tp": t_to}, device_id_type=MESH)

    def p_copy(step, block, c_from):
        return pltpu.make_async_remote_copy(
            src_ref=summed.at[block, (chip + step) % C], dst_ref=got.at[block, c_from], send_sem=p_ss.at[block, step - 1],
            recv_sem=p_rs.at[block, c_from], device_id=peer(step), device_id_type=MESH)

    for kind in kinds:
        own_copy(kind).start()
    halo_copy().start()
    for kind in kinds:
        for step in range(1, Y):
            y_copy(kind, step).start()
    chain_own((POOL,))
    chain_own(GU)
    chain_range((POOL,), 1, F)
    chain_range(GU, 1, Y)
    for step in range(1, S):
        share_copy(step, q).start()

    halo_copy().wait_recv()
    before = rms_scale(halo[...].astype(f32), gain_in[...]).astype(bf16).astype(f32)
    normed[pl.ds(0, margin), :] = jnp.where(t > 0, before, 0.0)
    normed[pl.ds(margin, rows), :] = rms_scale(tokens[...].astype(f32), gain_in[...]).astype(bf16).astype(f32)
    where = t * rows + lax.broadcasted_iota(jnp.int32, (rows, gc), 0)
    for step in range(1, S):
        share_copy(step, (q + step) % S).wait_recv()
    for group, span in enumerate(pool_spans):
        total = normed[:, group * gc : (group + 1) * gc]
        block = total[margin:]
        reach = 1
        while reach < span:
            total = total + pltpu.roll(total, reach, 0)
            reach *= 2
        gap = (total[margin:] / jnp.minimum(where + 1, span).astype(f32) - block).astype(bf16)
        mixed = jnp.dot(gap, pool_all[group], preferred_element_type=f32)
        after[:, group * gc : (group + 1) * gc] = mixed.astype(bf16).astype(f32)
    after[...] = tokens[...].astype(f32) + rms_scale(after[...], gain_out[...])
    whole = rms_scale(after[...], gain_ffn[...]).astype(bf16)
    for k in range(F):
        x_all[me, k] = whole[:, k * depth : (k + 1) * depth]
    for step in range(1, C):
        x_copy(step, chip).start()
    for step in range(1, T):
        x_across(step, chip, t).start()

    acc_g[...] = jnp.zeros_like(acc_g)
    acc_u[...] = jnp.zeros_like(acc_u)

    def times(lhs, rhs):
        return lax.dot_general(lhs, rhs, (((1,), (1,)), ((), ())), preferred_element_type=f32)

    def gate_up(origin):
        def body(g, carry):
            x = x_all[g, origin]
            at = pl.ds(pl.multiple_of(8 + g * rows, 8), rows)
            acc_g[at, :] += times(x, w_gu[origin, 0])
            acc_u[at, :] += times(x, w_gu[origin, 1])
            return carry
        lax.fori_loop(0, G, body, 0)

    ahead = Y * (1 + jnp.maximum(1, 2 * side))
    chain_range(GU, Y, ahead)
    chain_own((DN,))
    chain_range((DN,), 1, Y)
    for back in range(1, C):
        c = (chip + C - back) % C
        x_copy(back, c).wait_recv()
        for step in range(1, T):
            x_across(step, c, t).start()
    for c in range(C):
        for step in range(1, T):
            x_across(step, c, (t + step) % T).wait_recv()

    def gate_up_step(k, carry):
        @pl.when(k >= ahead)
        def _():
            chain(GU, k)
        gate_up(place(k)[1])
        return carry
    lax.fori_loop(0, F, gate_up_step, 0)
    chain_range((DN,), Y, ahead)

    taps = gate_taps.shape[0]

    def convolve(acc, taps_ref, g, keep):
        block = acc[pl.ds(pl.multiple_of(g * rows, 8), rows + 8), :]
        total = taps_ref[taps - 1 : taps, :] * block[8:]
        for back in range(1, taps):
            moved = pltpu.roll(block, back, 0)[8:]
            total = total + taps_ref[taps - 1 - back : taps - back, :] * jnp.where(keep >= back, moved, 0.0)
        return total

    def activate(g, carry):
        keep = (g % T) * rows + lax.broadcasted_iota(jnp.int32, (rows, cols), 0)
        hidden[g] = (gelu(convolve(acc_g, gate_taps, g, keep)) * convolve(acc_u, up_taps, g, keep)).astype(bf16)
        return carry

    lax.fori_loop(0, G, activate, 0)

    def down(block):
        def body(i, carry):
            step, c = i // C + 1, i % C
            t_to = (t + step) % T
            product = jnp.dot(hidden[c * T + t_to], w_d[block], preferred_element_type=f32)
            partial[block, t_to, c] = product.astype(bf16)
            return carry
        lax.fori_loop(0, G - C, body, 0)
        for step in range(1, T):
            s_copy(step, block, t).start()
        lax.fori_loop(G - C, G, body, 0)

    def add_up(block):
        for back in range(1, T):
            s_copy(back, block, (t + back) % T).wait_recv()

        def body(c, carry):
            total = partial[block, t, c].astype(f32)
            for back in range(1, T):
                total = total + swapped[block, (t + back) % T, c].astype(f32)
            summed[block, c] = total.astype(bf16)
            return carry
        lax.fori_loop(0, C, body, 0)
        for step in range(1, C):
            p_copy(step, block, chip).start()
        got[block, chip] = summed[block, chip]

    def down_step(k, carry):
        @pl.when(k >= ahead)
        def _():
            chain((DN,), k)
        down(place(k)[1])

        @pl.when(k > 0)
        def _():
            add_up(place(k - 1)[1])
        return carry
    lax.fori_loop(0, F, down_step, 0)
    add_up(place(F - 1)[1])

    def finish(block, carry):
        for step in range(1, C):
            p_copy(step, block, (chip + step) % C).wait_recv()
        return carry

    lax.fori_loop(0, F, finish, 0)
    for k in range(F):
        total = got[k, 0].astype(f32)
        for c in range(1, C):
            total = total + got[k, c].astype(f32)
        normed[pl.ds(0, rows), k * depth : (k + 1) * depth] = total
    out[...] = (after[...] + rms_scale(normed[pl.ds(0, rows), :], gain_last[...])).astype(bf16)

    halo_copy().wait_send()
    for step in range(1, S):
        share_copy(step, q).wait_send()
    for step in range(1, C):
        x_copy(step, chip).wait_send()
    for step in range(1, T):
        for c in range(C):
            x_across(step, c, t).wait_send()
    for kind in kinds:
        for step in range(1, Y):
            y_copy(kind, step).wait_send()

        def ended(origin, carry):
            @pl.when((origin // Y <= z) & (z + 1 < Z))
            def _():
                chain_copy(kind, origin, 1).wait_send()

            @pl.when((origin // Y >= z) & (z > 0))
            def _():
                chain_copy(kind, origin, -1).wait_send()
            return carry
        lax.fori_loop(0, F, ended, 0)

    def sent(block, carry):
        for step in range(1, T):
            s_copy(step, block, t).wait_send()
        for step in range(1, C):
            p_copy(step, block, chip).wait_send()
        return carry
    lax.fori_loop(0, F, sent, 0)


def solution(mesh):
    def shards(tokens, gain_in, pool, gain_out, gain_ffn, gate_w, up_w, gate_taps, up_taps, down_w, gain_last):
        rows, width = tokens.shape
        depth, columns = gate_w.shape
        plan = Plan(mesh, depth, width, columns)
        F, G, T, Y, Z, cols = plan.F, plan.G, plan.T, plan.Y, plan.Z, plan.cols
        groups, gc = pool.shape[0], pool.shape[2]
        C = G // T
        first = lax.axis_index("tp") * columns
        if plan.joined:
            first = first + (lax.axis_index("rep") * Y + lax.axis_index("fs") % Y) * cols
        gt = lax.dynamic_slice_in_dim(gate_taps, first, cols, 1)
        ut = lax.dynamic_slice_in_dim(up_taps, first, cols, 1)
        margin = max(pool_spans)
        vmem = pl.BlockSpec(memory_space=pltpu.VMEM)
        anywhere = pl.BlockSpec(memory_space=pl.ANY)
        dma = pltpu.SemaphoreType.DMA
        S = min(T, groups)
        V = pltpu.VMEM
        return pl.pallas_call(
            functools.partial(kernel, plan),
            out_shape=jax.ShapeDtypeStruct((rows, width), bf16),
            in_specs=[vmem, vmem, anywhere, vmem, vmem, anywhere, anywhere, anywhere, vmem, vmem, vmem],
            out_specs=vmem,
            scratch_shapes=[
                V((margin, width), bf16), V((groups, gc, gc), bf16), V((F, 2, cols, depth), bf16), V((F, cols, depth), bf16),
                V((G, F, rows, depth), bf16), V((margin + rows, width), f32), V((rows, width), f32),
                V((8 + G * rows, cols), f32), V((8 + G * rows, cols), f32), V((G, rows, cols), bf16),
                V((F, T, C, rows, depth), bf16), V((F, T, C, rows, depth), bf16), V((F, C, rows, depth), bf16), V((F, C, rows, depth), bf16),
                dma((4,)), dma((2,)), dma((4, max(Y - 1, 1))), dma((4, F)), dma((4, F)), dma((4, F)),
                dma((max(S - 1, 1),)), dma((S,)), dma((max(C - 1, 1),)), dma((G,)),
                dma((max(T - 1, 1), C)), dma((F, max(T - 1, 1))), dma((F, T)), dma((F, max(C - 1, 1))), dma((F, C)),
            ],
            compiler_params=pltpu.CompilerParams(has_side_effects=True, vmem_limit_bytes=61 * 2**20),
            name="layer",
        )(tokens, gain_in[None], pool, gain_out[None], gain_ffn[None], gate_w.T, up_w.T, down_w, gt, ut, gain_last[None])

    in_specs = (
        P(("rep", "fs", "tp"), None), P(), P(None, "fs", None), P(), P(),
        P("fs", "tp"), P("fs", "tp"), P(), P(), P("tp", "fs"), P(),
    )
    return jax.shard_map(shards, mesh=mesh, in_specs=in_specs, out_specs=P(("rep", "fs", "tp"), None), check_vma=False)
```

profile of v0, /device:TPU:0, one launch (start us, length us, event | category | flops | bytes accessed | tf_op | source)
XLA Modules:
  0.0 200.8 jit_solution(1656154453861352337)
XLA Ops:
  0.0 1.4 constant_dynamic-slice_fusion
  1.4 0.0 copy-start
  1.4 2.6 %copy.12 = bf16[256,2816]{0,1:T(8,128)(2,1)} copy(bf16[256,2816]{1,0:T(8,128)(2,1)} %param.16) | data formatting | bytes 2883584 | tf_op args[5]
  4.1 0.0 copy-done
  4.1 1.6 copy.13
  5.6 193.0 %layer.1 = bf16[192,2048]{1,0:T(8,128)(2,1)} custom-call(bf16[192,2048]{1,0:T(8,128)(2,1)} %tokens.1, f32[1,2048]{1,0:T(1,128)} %bitcast.8, bf16[4,64,512]{2,1,0:T(8,128)(2,1)} %pool.1, f32[1,2048]{1,0:T(1,128)} %bitcast.9, f32[1,2048]{1,0:T(1,128)} %bitcast.10, bf16[2816,256]{1,0:T(8,128)(2,1)} %bitcast.6, bf16[2816,256]{1,0:T(8,128)(2,1)} %bitcast.7, ...), custom_call_target="tpu_custom_call" | custom-call | tf_op jit(solution)/shard_map/layer/pallas_call | solution.py:368
  198.7 2.1 %copy.15 = bf16[192,2048]{1,0:T(8,128)(2,1)} copy(bf16[192,2048]{1,0:T(8,128)(2,1)} %layer.1) | data formatting | bytes 1572864
Async XLA Ops:
  1.4 2.7 %copy-start = (bf16[256,2816]{1,0:T(8,128)(2,1)S(1)}, bf16[256,2816]{1,0:T(8,128)(2,1)}, u32[]{:S(2)}) copy-start(bf16[256,2816]{1,0:T(8,128)(2,1)} %param.17) | copy-start | bytes 4325380
where the time goes:
time: 201 us
  Pallas kernels  193 us (96%)
  local copies, waits for them, and re-layouts  7.72 us (4%)
    pallas_call x1, Pallas kernels, shards(): pl.pallas_call(functools.partial(kernel, plan), out_shape=jax.ShapeDtypeS...  193 us
    unnamed x5, local copies, waits for them, and re-layouts  6.31 us

commit v1 on v0

--- a/solution.py
+++ b/solution.py
@@ -37,26 +37,34 @@
         self.G = self.T * self.n_sub
         self.cols = columns // self.n_sub
 
+    def pool_owners(self, groups):
+        S = min(self.T, groups)
+        PR = self.R if self.joined and groups % (self.R * S) == 0 else 1
+        return S, PR
+
 
 def kernel(
     plan, tokens, gain_in, pool, gain_out, gain_ffn, gate_t, up_t, down_w, gate_taps, up_taps, gain_last, out,
     halo, pool_all, w_gu, w_d, x_all, normed, after, acc_g, acc_u, hidden, partial, swapped, summed, got,
-    own_sem, halo_sem, y_ss, up_ss, dn_ss, piece_rs, share_ss, share_rs, x_ss, x_rs, f_ss, s_ss, s_rs, p_ss, p_rs,
+    own_sem, halo_sem, y_ss, up_ss, dn_ss, piece_rs, pz_ss, pz_rs, pp_ss, pp_rs, share_ss, share_rs,
+    x_ss, x_rs, f_ss, s_ss, s_rs, p_ss, p_rs,
 ):
     R, F, T, Y, Z, G, cols = plan.R, plan.F, plan.T, plan.Y, plan.Z, plan.G, plan.cols
     r, f, t = lax.axis_index("rep"), lax.axis_index("fs"), lax.axis_index("tp")
     z, y = f // Y, f % Y
     rows, width = tokens.shape
     depth = width // F
-    groups, gc = pool_all.shape[0], pool_all.shape[1]
+    groups, gc = pool_all.shape[0], pool_all.shape[3]
     slab = gc // F
-    S = min(T, groups)
-    GS = groups // S
+    S, PR = plan.pool_owners(groups)
+    PC = PR * Y
+    GS = groups // (S * PR)
     q = t % S
+    rp = r if PR > 1 else 0
     margin = halo.shape[0]
     C = G // T
-    POOL, GA, UP, DN = 0, 1, 2, 3
-    kinds = (POOL, GA, UP, DN)
+    GA, UP, DN, POOL = 0, 1, 2, 3
+    kinds = (GA, UP, DN)
     GU = (GA, UP)
 
     chip = r * Y + y if plan.joined else 0
@@ -73,14 +81,42 @@
         return pl.ds(pl.multiple_of(sub_of(y_to) * cols, 64 if cols % 64 == 0 else 8), cols)
 
     def slot(kind, origin):
-        if kind == POOL:
-            return pool_all.at[pl.ds(q * GS, GS), pl.ds(pl.multiple_of(origin * slab, slab), slab)]
         return w_d.at[origin] if kind == DN else w_gu.at[origin, kind - GA]
 
     def source(kind, y_to):
-        if kind == POOL:
-            return pool.at[pl.ds(q * GS, GS)]
         return (gate_t, up_t, down_w)[kind - GA].at[w_rows(y_to)]
+
+    def pool_groups(rp_of, q_of):
+        return pl.ds((rp_of * S + q_of) * GS, GS)
+
+    def pool_rows(y_of):
+        return pl.ds(pl.multiple_of(y_of * slab, slab), slab)
+
+    def pool_own():
+        return pltpu.make_async_copy(
+            pool.at[pool_groups(rp, q)], pool_all.at[pool_groups(rp, q), z, pool_rows(y)], own_sem.at[POOL])
+
+    def pool_z(step, z_from):
+        return pltpu.make_async_remote_copy(
+            src_ref=pool.at[pool_groups(rp, q)], dst_ref=pool_all.at[pool_groups(rp, q), z_from, pool_rows(y)],
+            send_sem=pz_ss.at[step - 1], recv_sem=pz_rs.at[z_from],
+            device_id={"fs": (z + step) % Z * Y + y}, device_id_type=MESH)
+
+    def pool_plane(step, from_pc):
+        block = pool_all.at[pool_groups(from_pc // Y, q), :, pool_rows(from_pc % Y)]
+        to = (rp * Y + y + step) % PC
+        device = {"fs": z * Y + to % Y}
+        if PR > 1:
+            device["rep"] = to // Y
+        return pltpu.make_async_remote_copy(
+            src_ref=block, dst_ref=block, send_sem=pp_ss.at[step - 1], recv_sem=pp_rs.at[from_pc],
+            device_id=device, device_id_type=MESH)
+
+    def share_copy(step, rp_of, q_from):
+        block = pool_all.at[pool_groups(rp_of, q_from)]
+        return pltpu.make_async_remote_copy(
+            src_ref=block, dst_ref=block, send_sem=share_ss.at[step - 1, rp_of], recv_sem=share_rs.at[rp_of, q_from],
+            device_id={"tp": t - q + (q + step) % S}, device_id_type=MESH)
 
     def own_copy(kind):
         return pltpu.make_async_copy(source(kind, y), slot(kind, f), own_sem.at[kind])
@@ -139,12 +175,6 @@
             src_ref=tokens.at[pl.ds(rows - margin, margin)], dst_ref=halo, send_sem=halo_sem.at[0],
             recv_sem=halo_sem.at[1], device_id={"tp": (t + 1) % T}, device_id_type=MESH)
 
-    def share_copy(step, q_from):
-        return pltpu.make_async_remote_copy(
-            src_ref=pool_all.at[pl.ds(q_from * GS, GS)], dst_ref=pool_all.at[pl.ds(q_from * GS, GS)],
-            send_sem=share_ss.at[step - 1], recv_sem=share_rs.at[q_from],
-            device_id={"tp": t - q + (q + step) % S}, device_id_type=MESH)
-
     def x_copy(step, c_from):
         g = c_from * T + t
         return pltpu.make_async_remote_copy(
@@ -168,26 +198,44 @@
             src_ref=summed.at[block, (chip + step) % C], dst_ref=got.at[block, c_from], send_sem=p_ss.at[block, step - 1],
             recv_sem=p_rs.at[block, c_from], device_id=peer(step), device_id_type=MESH)
 
+    pool_own().start()
     for kind in kinds:
         own_copy(kind).start()
+    near = [{"fs": (z + step) % Z * Y + y} for step in range(1, Z)]
+    near += [peer(step) for step in range(1, C)] if plan.joined else [{"fs": z * Y + (y + step) % Y} for step in range(1, Y)]
+    near += [{"tp": (t + step) % T} for step in range(1, T)]
+    barrier = pltpu.get_barrier_semaphore()
+    for device in near:
+        pl.semaphore_signal(barrier, inc=1, device_id=device, device_id_type=MESH)
+    pl.semaphore_wait(barrier, len(near))
+
+    for step in range(1, Z):
+        pool_z(step, z).start()
     halo_copy().start()
-    for kind in kinds:
+    for kind in GU:
         for step in range(1, Y):
             y_copy(kind, step).start()
-    chain_own((POOL,))
     chain_own(GU)
-    chain_range((POOL,), 1, F)
-    chain_range(GU, 1, Y)
-    for step in range(1, S):
-        share_copy(step, q).start()
-
+    normed[pl.ds(margin, rows), :] = rms_scale(tokens[...].astype(f32), gain_in[...]).astype(bf16).astype(f32)
     halo_copy().wait_recv()
     before = rms_scale(halo[...].astype(f32), gain_in[...]).astype(bf16).astype(f32)
     normed[pl.ds(0, margin), :] = jnp.where(t > 0, before, 0.0)
-    normed[pl.ds(margin, rows), :] = rms_scale(tokens[...].astype(f32), gain_in[...]).astype(bf16).astype(f32)
     where = t * rows + lax.broadcasted_iota(jnp.int32, (rows, gc), 0)
+
+    pool_own().wait()
+    for step in range(1, Z):
+        pool_z(step, (z + step) % Z).wait_recv()
+    for step in range(1, PC):
+        pool_plane(step, rp * Y + y).start()
+    chain_range(GU, 1, Y)
+    for step in range(1, PC):
+        pool_plane(step, (rp * Y + y + step) % PC).wait_recv()
     for step in range(1, S):
-        share_copy(step, (q + step) % S).wait_recv()
+        for rp_of in range(PR):
+            share_copy(step, rp_of, q).start()
+    for step in range(1, S):
+        for rp_of in range(PR):
+            share_copy(step, rp_of, (q + step) % S).wait_recv()
     for group, span in enumerate(pool_spans):
         total = normed[:, group * gc : (group + 1) * gc]
         block = total[margin:]
@@ -196,7 +244,7 @@
             total = total + pltpu.roll(total, reach, 0)
             reach *= 2
         gap = (total[margin:] / jnp.minimum(where + 1, span).astype(f32) - block).astype(bf16)
-        mixed = jnp.dot(gap, pool_all[group], preferred_element_type=f32)
+        mixed = jnp.dot(gap, pool_all[group].reshape(gc, gc), preferred_element_type=f32)
         after[:, group * gc : (group + 1) * gc] = mixed.astype(bf16).astype(f32)
     after[...] = tokens[...].astype(f32) + rms_scale(after[...], gain_out[...])
     whole = rms_scale(after[...], gain_ffn[...]).astype(bf16)
@@ -222,8 +270,11 @@
             return carry
         lax.fori_loop(0, G, body, 0)
 
-    ahead = Y * (1 + jnp.maximum(1, 2 * side))
-    chain_range(GU, Y, ahead)
+    early = jnp.where(side > 0, F, Y)
+    ahead = Y * (1 + 2 * side)
+    for step in range(1, Y):
+        y_copy(DN, step).start()
+    chain_range(GU, Y, early)
     chain_own((DN,))
     chain_range((DN,), 1, Y)
     for back in range(1, C):
@@ -236,7 +287,7 @@
             x_across(step, c, (t + step) % T).wait_recv()
 
     def gate_up_step(k, carry):
-        @pl.when(k >= ahead)
+        @pl.when(k >= early)
         def _():
             chain(GU, k)
         gate_up(place(k)[1])
@@ -291,10 +342,11 @@
     def down_step(k, carry):
         @pl.when(k >= ahead)
         def _():
+            add_up(place(k - 1)[1])
             chain((DN,), k)
         down(place(k)[1])
 
-        @pl.when(k > 0)
+        @pl.when((k > 0) & (k < ahead))
         def _():
             add_up(place(k - 1)[1])
         return carry
@@ -315,8 +367,13 @@
     out[...] = (after[...] + rms_scale(normed[pl.ds(0, rows), :], gain_last[...])).astype(bf16)
 
     halo_copy().wait_send()
+    for step in range(1, Z):
+        pool_z(step, z).wait_send()
+    for step in range(1, PC):
+        pool_plane(step, rp * Y + y).wait_send()
     for step in range(1, S):
-        share_copy(step, q).wait_send()
+        for rp_of in range(PR):
+            share_copy(step, rp_of, q).wait_send()
     for step in range(1, C):
         x_copy(step, chip).wait_send()
     for step in range(1, T):
@@ -363,7 +420,8 @@
         vmem = pl.BlockSpec(memory_space=pltpu.VMEM)
         anywhere = pl.BlockSpec(memory_space=pl.ANY)
         dma = pltpu.SemaphoreType.DMA
-        S = min(T, groups)
+        S, PR = plan.pool_owners(groups)
+        PC = PR * Y
         V = pltpu.VMEM
         return pl.pallas_call(
             functools.partial(kernel, plan),
@@ -371,15 +429,15 @@
             in_specs=[vmem, vmem, anywhere, vmem, vmem, anywhere, anywhere, anywhere, vmem, vmem, vmem],
             out_specs=vmem,
             scratch_shapes=[
-                V((margin, width), bf16), V((groups, gc, gc), bf16), V((F, 2, cols, depth), bf16), V((F, cols, depth), bf16),
+                V((margin, width), bf16), V((groups, Z, gc // Z, gc), bf16), V((F, 2, cols, depth), bf16), V((F, cols, depth), bf16),
                 V((G, F, rows, depth), bf16), V((margin + rows, width), f32), V((rows, width), f32),
                 V((8 + G * rows, cols), f32), V((8 + G * rows, cols), f32), V((G, rows, cols), bf16),
                 V((F, T, C, rows, depth), bf16), V((F, T, C, rows, depth), bf16), V((F, C, rows, depth), bf16), V((F, C, rows, depth), bf16),
-                dma((4,)), dma((2,)), dma((4, max(Y - 1, 1))), dma((4, F)), dma((4, F)), dma((4, F)),
-                dma((max(S - 1, 1),)), dma((S,)), dma((max(C - 1, 1),)), dma((G,)),
+                dma((4,)), dma((2,)), dma((3, max(Y - 1, 1))), dma((3, F)), dma((3, F)), dma((3, F)),
+                dma((max(Z - 1, 1),)), dma((Z,)), dma((max(PC - 1, 1),)), dma((PC,)), dma((max(S - 1, 1), PR)), dma((PR, S)), dma((max(C - 1, 1),)), dma((G,)),
                 dma((max(T - 1, 1), C)), dma((F, max(T - 1, 1))), dma((F, T)), dma((F, max(C - 1, 1))), dma((F, C)),
             ],
-            compiler_params=pltpu.CompilerParams(has_side_effects=True, vmem_limit_bytes=61 * 2**20),
+            compiler_params=pltpu.CompilerParams(has_side_effects=True, collective_id=0, vmem_limit_bytes=61 * 2**20),
             name="layer",
         )(tokens, gain_in[None], pool, gain_out[None], gain_ffn[None], gate_w.T, up_w.T, down_w, gt, ut, gain_last[None])
 

time: 201 us -> 173 us (0.86)
  Pallas kernels: 193 us -> 165 us
    pallas_call x1, Pallas kernels: 193 us -> 165 us  [shards(): pl.pallas_call(functools.partial(kernel, plan), out_shape=jax.ShapeDtypeS...]
where the time goes in v1:
time: 173 us
  Pallas kernels  165 us (95%)
  local copies, waits for them, and re-layouts  7.72 us (4%)
    pallas_call x1, Pallas kernels, shards(): pl.pallas_call(functools.partial(kernel, plan), out_shape=jax.ShapeDtypeS...  165 us
    unnamed x5, local copies, waits for them, and re-layouts  6.31 us

profile of v1, /device:TPU:0, one launch (start us, length us, event | category | flops | bytes accessed | tf_op | source)
XLA Modules:
  0.0 173.1 jit_solution(12193199272311781017)
XLA Ops:
  0.0 1.4 constant_dynamic-slice_fusion
  1.4 0.0 copy-start
  1.4 2.6 %copy.12 = bf16[256,2816]{0,1:T(8,128)(2,1)} copy(bf16[256,2816]{1,0:T(8,128)(2,1)} %param.16) | data formatting | bytes 2883584 | tf_op args[5]
  4.1 0.0 copy-done
  4.1 1.6 copy.13
  5.6 165.3 %layer.1 = bf16[192,2048]{1,0:T(8,128)(2,1)} custom-call(bf16[192,2048]{1,0:T(8,128)(2,1)} %tokens.1, f32[1,2048]{1,0:T(1,128)} %bitcast.8, bf16[4,64,512]{2,1,0:T(8,128)(2,1)} %pool.1, f32[1,2048]{1,0:T(1,128)} %bitcast.9, f32[1,2048]{1,0:T(1,128)} %bitcast.10, bf16[2816,256]{1,0:T(8,128)(2,1)} %bitcast.6, bf16[2816,256]{1,0:T(8,128)(2,1)} %bitcast.7, ...), custom_call_target="tpu_custom_call" | custom-call | tf_op jit(solution)/shard_map/layer/pallas_call | solution.py:426
  171.0 2.1 %copy.15 = bf16[192,2048]{1,0:T(8,128)(2,1)} copy(bf16[192,2048]{1,0:T(8,128)(2,1)} %layer.1) | data formatting | bytes 1572864
Async XLA Ops:
  1.4 2.7 %copy-start = (bf16[256,2816]{1,0:T(8,128)(2,1)S(1)}, bf16[256,2816]{1,0:T(8,128)(2,1)}, u32[]{:S(2)}) copy-start(bf16[256,2816]{1,0:T(8,128)(2,1)} %param.17) | copy-start | bytes 4325380

commit v2 on v1

--- a/solution.py
+++ b/solution.py
@@ -10,6 +10,7 @@
 MESH = pl.DeviceIdType.MESH
 pool_spans = (2, 4, 8, 16)
 rms_eps = 1e-06
+lanes = 128
 weight_budget = 24 * 2**20
 f32 = jnp.float32
 bf16 = jnp.bfloat16
@@ -32,10 +33,15 @@
         while self.F % self.Y:
             self.Y -= 1
         self.Z = self.F // self.Y
-        self.joined = 3 * width * columns * 2 > weight_budget
+        self.joined = 3 * width * columns * 2 > weight_budget and columns % lanes == 0
         self.n_sub = self.R * self.Y if self.joined else 1
         self.G = self.T * self.n_sub
-        self.cols = columns // self.n_sub
+        self.tiles = columns // lanes
+        self.cols = -(-self.tiles // self.n_sub) * lanes if self.joined else columns
+        self.small = self.tiles // self.n_sub * lanes if self.joined else columns
+
+    def first_tile(self, sub, t):
+        return (sub * self.tiles + self.n_sub // 2 * ((t + 1) % 2)) // self.n_sub
 
     def pool_owners(self, groups):
         S = min(self.T, groups)
@@ -44,7 +50,7 @@
 
 
 def kernel(
-    plan, tokens, gain_in, pool, gain_out, gain_ffn, gate_t, up_t, down_w, gate_taps, up_taps, gain_last, out,
+    plan, tokens, gain_in, pool, gain_out, gain_ffn, gate_w, up_w, down_w, gate_taps, up_taps, gain_last, out,
     halo, pool_all, w_gu, w_d, x_all, normed, after, acc_g, acc_u, hidden, partial, swapped, summed, got,
     own_sem, halo_sem, y_ss, up_ss, dn_ss, piece_rs, pz_ss, pz_rs, pp_ss, pp_rs, share_ss, share_rs,
     x_ss, x_rs, f_ss, s_ss, s_rs, p_ss, p_rs,
@@ -77,14 +83,32 @@
     def sub_of(y_to):
         return r * Y + y_to if plan.joined else 0
 
-    def w_rows(y_to):
-        return pl.ds(pl.multiple_of(sub_of(y_to) * cols, 64 if cols % 64 == 0 else 8), cols)
-
-    def slot(kind, origin):
-        return w_d.at[origin] if kind == DN else w_gu.at[origin, kind - GA]
-
-    def source(kind, y_to):
-        return (gate_t, up_t, down_w)[kind - GA].at[w_rows(y_to)]
+    def by_size(y_to, run):
+        if plan.small == cols:
+            run(cols)
+            return
+        tiles = plan.first_tile(sub_of(y_to) + 1, t) - plan.first_tile(sub_of(y_to), t)
+
+        @pl.when(tiles * lanes == cols)
+        def _():
+            run(cols)
+
+        @pl.when(tiles * lanes != cols)
+        def _():
+            run(plan.small)
+
+    def columns_of(y_to, size):
+        if not plan.joined:
+            return pl.ds(0, size)
+        return pl.ds(pl.multiple_of(plan.first_tile(sub_of(y_to), t) * lanes, lanes), size)
+
+    def slot(kind, origin, size):
+        return w_d.at[origin, pl.ds(0, size)] if kind == DN else w_gu.at[origin, kind - GA, :, pl.ds(0, size)]
+
+    def source(kind, y_to, size):
+        if kind == DN:
+            return down_w.at[columns_of(y_to, size)]
+        return (gate_w, up_w)[kind - GA].at[:, columns_of(y_to, size)]
 
     def pool_groups(rp_of, q_of):
         return pl.ds((rp_of * S + q_of) * GS, GS)
@@ -118,31 +142,33 @@
             src_ref=block, dst_ref=block, send_sem=share_ss.at[step - 1, rp_of], recv_sem=share_rs.at[rp_of, q_from],
             device_id={"tp": t - q + (q + step) % S}, device_id_type=MESH)
 
-    def own_copy(kind):
-        return pltpu.make_async_copy(source(kind, y), slot(kind, f), own_sem.at[kind])
-
-    def y_copy(kind, step):
+    def own_copy(kind, size):
+        return pltpu.make_async_copy(source(kind, y, size), slot(kind, f, size), own_sem.at[kind])
+
+    def y_copy(kind, step, size):
         y_to = (y + step) % Y
         return pltpu.make_async_remote_copy(
-            src_ref=source(kind, y_to), dst_ref=slot(kind, f), send_sem=y_ss.at[kind, step - 1],
+            src_ref=source(kind, y_to, size), dst_ref=slot(kind, f, size), send_sem=y_ss.at[kind, step - 1],
             recv_sem=piece_rs.at[kind, f], device_id={"fs": z * Y + y_to}, device_id_type=MESH)
 
-    def chain_copy(kind, origin, dz):
-        return pltpu.make_async_remote_copy(
-            src_ref=slot(kind, origin), dst_ref=slot(kind, origin), send_sem=(up_ss if dz > 0 else dn_ss).at[kind, origin],
+    def chain_copy(kind, origin, dz, size):
+        block = slot(kind, origin, size)
+        return pltpu.make_async_remote_copy(
+            src_ref=block, dst_ref=block, send_sem=(up_ss if dz > 0 else dn_ss).at[kind, origin],
             recv_sem=piece_rs.at[kind, origin], device_id={"fs": (z + dz) * Y + y}, device_id_type=MESH)
 
-    def arrived(kind, origin):
-        chain_copy(kind, origin, 1).wait_recv()
-
-    def pass_on(kind, origin, z0):
+    def pass_on(kind, origin, z0, size):
         @pl.when((z0 <= z) & (z + 1 < Z))
         def _():
-            chain_copy(kind, origin, 1).start()
+            chain_copy(kind, origin, 1, size).start()
 
         @pl.when((z0 >= z) & (z > 0))
         def _():
-            chain_copy(kind, origin, -1).start()
+            chain_copy(kind, origin, -1, size).start()
+
+    def y_start(kinds_now):
+        for step in range(1, Y):
+            by_size((y + step) % Y, lambda size: [y_copy(kind, step, size).start() for kind in kinds_now])
 
     side = jnp.minimum(z, Z - 1 - z)
 
@@ -155,14 +181,19 @@
 
     def chain(kinds_now, k):
         z0, origin = place(k)
-        for kind in kinds_now:
-            arrived(kind, origin)
-            pass_on(kind, origin, z0)
+
+        def run(size):
+            for kind in kinds_now:
+                chain_copy(kind, origin, 1, size).wait_recv()
+                pass_on(kind, origin, z0, size)
+        by_size(y, run)
 
     def chain_own(kinds_now):
-        for kind in kinds_now:
-            own_copy(kind).wait()
-            pass_on(kind, f, z)
+        def run(size):
+            for kind in kinds_now:
+                own_copy(kind, size).wait()
+                pass_on(kind, f, z, size)
+        by_size(y, run)
 
     def chain_range(kinds_now, first, last):
         def body(k, carry):
@@ -190,7 +221,7 @@
     def s_copy(step, block, t_from):
         t_to = (t + step) % T
         return pltpu.make_async_remote_copy(
-            src_ref=partial.at[block, t_to], dst_ref=swapped.at[block, t_from], send_sem=s_ss.at[block, step - 1],
+            src_ref=partial.at[block, t_to], dst_ref=swapped.at[block, step - 1], send_sem=s_ss.at[block, step - 1],
             recv_sem=s_rs.at[block, t_from], device_id={"tp": t_to}, device_id_type=MESH)
 
     def p_copy(step, block, c_from):
@@ -199,22 +230,24 @@
             recv_sem=p_rs.at[block, c_from], device_id=peer(step), device_id_type=MESH)
 
     pool_own().start()
-    for kind in kinds:
-        own_copy(kind).start()
+    by_size(y, lambda size: [own_copy(kind, size).start() for kind in kinds])
     near = [{"fs": (z + step) % Z * Y + y} for step in range(1, Z)]
     near += [peer(step) for step in range(1, C)] if plan.joined else [{"fs": z * Y + (y + step) % Y} for step in range(1, Y)]
     near += [{"tp": (t + step) % T} for step in range(1, T)]
     barrier = pltpu.get_barrier_semaphore()
     for device in near:
         pl.semaphore_signal(barrier, inc=1, device_id=device, device_id_type=MESH)
+    def blank(size):
+        if size < cols:
+            w_gu[:, :, :, size:cols] = jnp.zeros((F, 2, depth, cols - size), bf16)
+            w_d[:, size:cols] = jnp.zeros((F, cols - size, depth), bf16)
+    by_size(y, blank)
     pl.semaphore_wait(barrier, len(near))
 
     for step in range(1, Z):
         pool_z(step, z).start()
     halo_copy().start()
-    for kind in GU:
-        for step in range(1, Y):
-            y_copy(kind, step).start()
+    y_start(GU)
     chain_own(GU)
     normed[pl.ds(margin, rows), :] = rms_scale(tokens[...].astype(f32), gain_in[...]).astype(bf16).astype(f32)
     halo_copy().wait_recv()
@@ -259,7 +292,7 @@
     acc_u[...] = jnp.zeros_like(acc_u)
 
     def times(lhs, rhs):
-        return lax.dot_general(lhs, rhs, (((1,), (1,)), ((), ())), preferred_element_type=f32)
+        return jnp.dot(lhs, rhs, preferred_element_type=f32)
 
     def gate_up(origin):
         def body(g, carry):
@@ -272,8 +305,7 @@
 
     early = jnp.where(side > 0, F, Y)
     ahead = Y * (1 + 2 * side)
-    for step in range(1, Y):
-        y_copy(DN, step).start()
+    y_start((DN,))
     chain_range(GU, Y, early)
     chain_own((DN,))
     chain_range((DN,), 1, Y)
@@ -296,13 +328,14 @@
     chain_range((DN,), Y, ahead)
 
     taps = gate_taps.shape[0]
+    window = pl.ds(pl.multiple_of(t * plan.tiles * lanes + plan.first_tile(sub_of(y), t) * lanes, lanes), cols) if plan.joined else slice(None)
 
     def convolve(acc, taps_ref, g, keep):
         block = acc[pl.ds(pl.multiple_of(g * rows, 8), rows + 8), :]
-        total = taps_ref[taps - 1 : taps, :] * block[8:]
+        total = taps_ref[taps - 1 : taps, window] * block[8:]
         for back in range(1, taps):
             moved = pltpu.roll(block, back, 0)[8:]
-            total = total + taps_ref[taps - 1 - back : taps - back, :] * jnp.where(keep >= back, moved, 0.0)
+            total = total + taps_ref[taps - 1 - back : taps - back, window] * jnp.where(keep >= back, moved, 0.0)
         return total
 
     def activate(g, carry):
@@ -331,7 +364,7 @@
         def body(c, carry):
             total = partial[block, t, c].astype(f32)
             for back in range(1, T):
-                total = total + swapped[block, (t + back) % T, c].astype(f32)
+                total = total + swapped[block, T - 1 - back, c].astype(f32)
             summed[block, c] = total.astype(bf16)
             return carry
         lax.fori_loop(0, C, body, 0)
@@ -379,20 +412,22 @@
     for step in range(1, T):
         for c in range(C):
             x_across(step, c, t).wait_send()
-    for kind in kinds:
-        for step in range(1, Y):
-            y_copy(kind, step).wait_send()
-
-        def ended(origin, carry):
-            @pl.when((origin // Y <= z) & (z + 1 < Z))
-            def _():
-                chain_copy(kind, origin, 1).wait_send()
-
-            @pl.when((origin // Y >= z) & (z > 0))
-            def _():
-                chain_copy(kind, origin, -1).wait_send()
-            return carry
-        lax.fori_loop(0, F, ended, 0)
+    for step in range(1, Y):
+        by_size((y + step) % Y, lambda size: [y_copy(kind, step, size).wait_send() for kind in kinds])
+
+    def all_ended(size):
+        for kind in kinds:
+            def ended(origin, carry):
+                @pl.when((origin // Y <= z) & (z + 1 < Z))
+                def _():
+                    chain_copy(kind, origin, 1, size).wait_send()
+
+                @pl.when((origin // Y >= z) & (z > 0))
+                def _():
+                    chain_copy(kind, origin, -1, size).wait_send()
+                return carry
+            lax.fori_loop(0, F, ended, 0)
+    by_size(y, all_ended)
 
     def sent(block, carry):
         for step in range(1, T):
@@ -411,11 +446,9 @@
         F, G, T, Y, Z, cols = plan.F, plan.G, plan.T, plan.Y, plan.Z, plan.cols
         groups, gc = pool.shape[0], pool.shape[2]
         C = G // T
-        first = lax.axis_index("tp") * columns
-        if plan.joined:
-            first = first + (lax.axis_index("rep") * Y + lax.axis_index("fs") % Y) * cols
-        gt = lax.dynamic_slice_in_dim(gate_taps, first, cols, 1)
-        ut = lax.dynamic_slice_in_dim(up_taps, first, cols, 1)
+        gt, ut = gate_taps, up_taps
+        if not plan.joined:
+            gt, ut = (lax.dynamic_slice_in_dim(v, lax.axis_index("tp") * columns, columns, 1) for v in (gate_taps, up_taps))
         margin = max(pool_spans)
         vmem = pl.BlockSpec(memory_space=pltpu.VMEM)
         anywhere = pl.BlockSpec(memory_space=pl.ANY)
@@ -429,17 +462,17 @@
             in_specs=[vmem, vmem, anywhere, vmem, vmem, anywhere, anywhere, anywhere, vmem, vmem, vmem],
             out_specs=vmem,
             scratch_shapes=[
-                V((margin, width), bf16), V((groups, Z, gc // Z, gc), bf16), V((F, 2, cols, depth), bf16), V((F, cols, depth), bf16),
+                V((margin, width), bf16), V((groups, Z, gc // Z, gc), bf16), V((F, 2, depth, cols), bf16), V((F, cols, depth), bf16),
                 V((G, F, rows, depth), bf16), V((margin + rows, width), f32), V((rows, width), f32),
                 V((8 + G * rows, cols), f32), V((8 + G * rows, cols), f32), V((G, rows, cols), bf16),
-                V((F, T, C, rows, depth), bf16), V((F, T, C, rows, depth), bf16), V((F, C, rows, depth), bf16), V((F, C, rows, depth), bf16),
+                V((F, T, C, rows, depth), bf16), V((F, max(T - 1, 1), C, rows, depth), bf16), V((F, C, rows, depth), bf16), V((F, C, rows, depth), bf16),
                 dma((4,)), dma((2,)), dma((3, max(Y - 1, 1))), dma((3, F)), dma((3, F)), dma((3, F)),
                 dma((max(Z - 1, 1),)), dma((Z,)), dma((max(PC - 1, 1),)), dma((PC,)), dma((max(S - 1, 1), PR)), dma((PR, S)), dma((max(C - 1, 1),)), dma((G,)),
                 dma((max(T - 1, 1), C)), dma((F, max(T - 1, 1))), dma((F, T)), dma((F, max(C - 1, 1))), dma((F, C)),
             ],
-            compiler_params=pltpu.CompilerParams(has_side_effects=True, collective_id=0, vmem_limit_bytes=61 * 2**20),
+            compiler_params=pltpu.CompilerParams(has_side_effects=True, collective_id=0, vmem_limit_bytes=52 * 2**20),
             name="layer",
-        )(tokens, gain_in[None], pool, gain_out[None], gain_ffn[None], gate_w.T, up_w.T, down_w, gt, ut, gain_last[None])
+        )(tokens, gain_in[None], pool, gain_out[None], gain_ffn[None], gate_w, up_w, down_w, gt, ut, gain_last[None])
 
     in_specs = (
         P(("rep", "fs", "tp"), None), P(), P(None, "fs", None), P(), P(),

time: 173 us -> 172 us (level)
    unnamed x5 -> x15, local copies, waits for them, and re-layouts: 6.31 us -> 6.4 us
where the time goes in v2:
time: 172 us; the launch traced here: 171 us
  Pallas kernels  165 us (96%)
  local copies, waits for them, and re-layouts  6.4 us (4%)
    pallas_call x1, Pallas kernels, shards(): pl.pallas_call(functools.partial(kernel, plan), out_shape=jax.ShapeDtypeS...  165 us
    unnamed x15, local copies, waits for them, and re-layouts  6.4 us

profile of v2, /device:TPU:0, one launch (start us, length us, event | category | flops | bytes accessed | tf_op | source)
XLA Modules:
  0.0 171.1 jit_solution(4478682227141685144)
XLA Ops:
  0.0 0.0 copy-start
  0.0 0.9 copy-done
  1.0 0.0 copy-start.1
  1.0 0.9 copy-done.1
  1.8 0.0 copy-start.2
  1.8 0.9 copy-done.2
  2.7 0.0 copy-start.3
  2.7 0.7 copy-done.3
  3.4 0.0 copy-start.4
  3.4 0.7 copy-done.4
  4.1 0.0 copy-start.5
  4.1 0.7 copy-done.5
  4.8 0.0 copy-start.6
  4.8 0.7 copy-done.6
  5.5 164.7 %layer.1 = bf16[192,2048]{1,0:T(8,128)(2,1)S(1)} custom-call(bf16[192,2048]{1,0:T(8,128)(2,1)} %tokens.1, f32[1,2048]{1,0:T(1,128)S(1)} %bitcast.4, bf16[4,64,512]{2,1,0:T(8,128)(2,1)S(1)} %copy-done, f32[1,2048]{1,0:T(1,128)S(1)} %bitcast.5, f32[1,2048]{1,0:T(1,128)S(1)} %bitcast.6, bf16[256,2816]{1,0:T(8,128)(2,1)} %gate_w.1, bf16[256,2816]{1,0:T(8,128)(2,1)} %up_w.1, ...), custom_call_target="tpu_custom_call" | custom-call | tf_op jit(solution)/shard_map/layer/pallas_call | solution.py:459
  170.2 0.9 copy.13
Async XLA Ops:
  0.0 0.9 copy-start
  1.0 0.9 copy-start.1
  1.8 0.9 copy-start.2
  2.7 0.7 copy-start.3
  3.4 0.7 copy-start.4
  4.1 0.7 copy-start.5
  4.8 0.7 copy-start.6

commit v3 on v2

--- a/solution.py
+++ b/solution.py
@@ -40,6 +40,9 @@
         self.cols = -(-self.tiles // self.n_sub) * lanes if self.joined else columns
         self.small = self.tiles // self.n_sub * lanes if self.joined else columns
 
+    def halves(self, depth):
+        return 2 if depth % (2 * lanes) == 0 else 1
+
     def first_tile(self, sub, t):
         return (sub * self.tiles + self.n_sub // 2 * ((t + 1) % 2)) // self.n_sub
 
@@ -50,9 +53,10 @@
 
 
 def kernel(
-    plan, tokens, gain_in, pool, gain_out, gain_ffn, gate_w, up_w, down_w, gate_taps, up_taps, gain_last, out,
+    plan, tokens_hbm, gain_in_hbm, pool, gain_out_hbm, gain_ffn_hbm, gate_w, up_w, down_w, gate_taps_hbm, up_taps_hbm, gain_last_hbm, out,
+    tokens, gain_in, gain_out, gain_ffn, gate_taps, up_taps, gain_last,
     halo, pool_all, w_gu, w_d, x_all, normed, after, acc_g, acc_u, hidden, partial, swapped, summed, got,
-    own_sem, halo_sem, y_ss, up_ss, dn_ss, piece_rs, pz_ss, pz_rs, pp_ss, pp_rs, share_ss, share_rs,
+    in_sem, own_sem, halo_sem, y_ss, up_ss, dn_ss, piece_rs, pz_ss, pz_rs, pp_ss, pp_rs, share_ss, share_rs,
     x_ss, x_rs, f_ss, s_ss, s_rs, p_ss, p_rs,
 ):
     R, F, T, Y, Z, G, cols = plan.R, plan.F, plan.T, plan.Y, plan.Z, plan.G, plan.cols
@@ -69,9 +73,13 @@
     rp = r if PR > 1 else 0
     margin = halo.shape[0]
     C = G // T
-    GA, UP, DN, POOL = 0, 1, 2, 3
-    kinds = (GA, UP, DN)
+    H = plan.halves(depth)
+    half = depth // H
+    GA, UP, DN = 0, 1, 2
     GU = (GA, UP)
+    DNS = tuple(range(DN, DN + H))
+    kinds = GU + DNS
+    POOL = DN + H
 
     chip = r * Y + y if plan.joined else 0
     me = chip * T + t
@@ -102,12 +110,17 @@
             return pl.ds(0, size)
         return pl.ds(pl.multiple_of(plan.first_tile(sub_of(y_to), t) * lanes, lanes), size)
 
+    def part(h):
+        return pl.ds(0, depth) if h is None else pl.ds(h * half, half)
+
     def slot(kind, origin, size):
-        return w_d.at[origin, pl.ds(0, size)] if kind == DN else w_gu.at[origin, kind - GA, :, pl.ds(0, size)]
+        if kind in DNS:
+            return w_d.at[origin, pl.ds(0, size), part(kind - DN)]
+        return w_gu.at[origin, kind - GA, :, pl.ds(0, size)]
 
     def source(kind, y_to, size):
-        if kind == DN:
-            return down_w.at[columns_of(y_to, size)]
+        if kind in DNS:
+            return down_w.at[columns_of(y_to, size), part(kind - DN)]
         return (gate_w, up_w)[kind - GA].at[:, columns_of(y_to, size)]
 
     def pool_groups(rp_of, q_of):
@@ -203,7 +216,7 @@
 
     def halo_copy():
         return pltpu.make_async_remote_copy(
-            src_ref=tokens.at[pl.ds(rows - margin, margin)], dst_ref=halo, send_sem=halo_sem.at[0],
+            src_ref=tokens_hbm.at[pl.ds(rows - margin, margin)], dst_ref=halo, send_sem=halo_sem.at[0],
             recv_sem=halo_sem.at[1], device_id={"tp": (t + 1) % T}, device_id_type=MESH)
 
     def x_copy(step, c_from):
@@ -218,17 +231,31 @@
             src_ref=x_all.at[g], dst_ref=x_all.at[g], send_sem=f_ss.at[step - 1, c],
             recv_sem=x_rs.at[g], device_id={"tp": (t + step) % T}, device_id_type=MESH)
 
-    def s_copy(step, block, t_from):
+    def flag(block, h):
+        return block if h is None else F + h
+
+    def s_copy(step, block, t_from, h=None):
         t_to = (t + step) % T
         return pltpu.make_async_remote_copy(
-            src_ref=partial.at[block, t_to], dst_ref=swapped.at[block, step - 1], send_sem=s_ss.at[block, step - 1],
-            recv_sem=s_rs.at[block, t_from], device_id={"tp": t_to}, device_id_type=MESH)
-
-    def p_copy(step, block, c_from):
-        return pltpu.make_async_remote_copy(
-            src_ref=summed.at[block, (chip + step) % C], dst_ref=got.at[block, c_from], send_sem=p_ss.at[block, step - 1],
-            recv_sem=p_rs.at[block, c_from], device_id=peer(step), device_id_type=MESH)
-
+            src_ref=partial.at[block, t_to, :, :, part(h)], dst_ref=swapped.at[block, step - 1, :, :, part(h)],
+            send_sem=s_ss.at[flag(block, h), step - 1], recv_sem=s_rs.at[flag(block, h), t_from],
+            device_id={"tp": t_to}, device_id_type=MESH)
+
+    def p_copy(step, block, c_from, h=None):
+        return pltpu.make_async_remote_copy(
+            src_ref=summed.at[block, (chip + step) % C, :, part(h)], dst_ref=got.at[block, c_from, :, part(h)],
+            send_sem=p_ss.at[flag(block, h), step - 1], recv_sem=p_rs.at[flag(block, h), c_from],
+            device_id=peer(step), device_id_type=MESH)
+
+    def last_block(y_of):
+        return place(F - 1)[0] * Y + (y_of + (F - 1) % Y) % Y
+
+    staged = [
+        pltpu.make_async_copy(source_ref, held, in_sem.at[k]) for k, (source_ref, held) in enumerate((
+            (tokens_hbm, tokens), (gain_in_hbm, gain_in), (gain_out_hbm, gain_out), (gain_ffn_hbm, gain_ffn),
+            (gate_taps_hbm, gate_taps), (up_taps_hbm, up_taps), (gain_last_hbm, gain_last)))]
+    staged[0].start()
+    staged[1].start()
     pool_own().start()
     by_size(y, lambda size: [own_copy(kind, size).start() for kind in kinds])
     near = [{"fs": (z + step) % Z * Y + y} for step in range(1, Z)]
@@ -249,6 +276,10 @@
     halo_copy().start()
     y_start(GU)
     chain_own(GU)
+    for copy in staged[2:]:
+        copy.start()
+    for copy in staged:
+        copy.wait()
     normed[pl.ds(margin, rows), :] = rms_scale(tokens[...].astype(f32), gain_in[...]).astype(bf16).astype(f32)
     halo_copy().wait_recv()
     before = rms_scale(halo[...].astype(f32), gain_in[...]).astype(bf16).astype(f32)
@@ -305,10 +336,10 @@
 
     early = jnp.where(side > 0, F, Y)
     ahead = Y * (1 + 2 * side)
-    y_start((DN,))
+    y_start(DNS)
     chain_range(GU, Y, early)
-    chain_own((DN,))
-    chain_range((DN,), 1, Y)
+    chain_own(DNS)
+    chain_range(DNS, 1, Y)
     for back in range(1, C):
         c = (chip + C - back) % C
         x_copy(back, c).wait_recv()
@@ -325,7 +356,7 @@
         gate_up(place(k)[1])
         return carry
     lax.fori_loop(0, F, gate_up_step, 0)
-    chain_range((DN,), Y, ahead)
+    chain_range(DNS, Y, jnp.minimum(ahead, F - 1))
 
     taps = gate_taps.shape[0]
     window = pl.ds(pl.multiple_of(t * plan.tiles * lanes + plan.first_tile(sub_of(y), t) * lanes, lanes), cols) if plan.joined else slice(None)
@@ -345,53 +376,65 @@
 
     lax.fori_loop(0, G, activate, 0)
 
-    def down(block):
+    def down(block, h=None):
         def body(i, carry):
             step, c = i // C + 1, i % C
             t_to = (t + step) % T
-            product = jnp.dot(hidden[c * T + t_to], w_d[block], preferred_element_type=f32)
-            partial[block, t_to, c] = product.astype(bf16)
+            product = jnp.dot(hidden[c * T + t_to], w_d[block, :, part(h)], preferred_element_type=f32)
+            partial[block, t_to, c, :, part(h)] = product.astype(bf16)
             return carry
         lax.fori_loop(0, G - C, body, 0)
         for step in range(1, T):
-            s_copy(step, block, t).start()
+            s_copy(step, block, t, h).start()
         lax.fori_loop(G - C, G, body, 0)
 
-    def add_up(block):
+    def add_up(block, h=None):
         for back in range(1, T):
-            s_copy(back, block, (t + back) % T).wait_recv()
+            s_copy(back, block, (t + back) % T, h).wait_recv()
 
         def body(c, carry):
-            total = partial[block, t, c].astype(f32)
+            total = partial[block, t, c, :, part(h)].astype(f32)
             for back in range(1, T):
-                total = total + swapped[block, T - 1 - back, c].astype(f32)
-            summed[block, c] = total.astype(bf16)
+                total = total + swapped[block, T - 1 - back, c, :, part(h)].astype(f32)
+            summed[block, c, :, part(h)] = total.astype(bf16)
             return carry
         lax.fori_loop(0, C, body, 0)
         for step in range(1, C):
-            p_copy(step, block, chip).start()
-        got[block, chip] = summed[block, chip]
+            p_copy(step, block, chip, h).start()
+        got[block, chip, :, part(h)] = summed[block, chip, :, part(h)]
 
     def down_step(k, carry):
         @pl.when(k >= ahead)
         def _():
             add_up(place(k - 1)[1])
-            chain((DN,), k)
+            chain(DNS, k)
         down(place(k)[1])
 
         @pl.when((k > 0) & (k < ahead))
         def _():
             add_up(place(k - 1)[1])
         return carry
-    lax.fori_loop(0, F, down_step, 0)
-    add_up(place(F - 1)[1])
+    lax.fori_loop(0, F - 1, down_step, 0)
+    if F > 1:
+        add_up(place(F - 2)[1])
+    for h in range(H):
+        if F > Y:
+            chain((DNS[h],), F - 1)
+        down(last_block(y), h)
+        add_up(last_block(y), h)
 
     def finish(block, carry):
         for step in range(1, C):
-            p_copy(step, block, (chip + step) % C).wait_recv()
+            @pl.when(block != last_block((chip + step) % C % Y))
+            def _():
+                p_copy(step, block, (chip + step) % C).wait_recv()
         return carry
 
     lax.fori_loop(0, F, finish, 0)
+    for step in range(1, C):
+        for h in range(H):
+            c_from = (chip + step) % C
+            p_copy(step, last_block(c_from % Y), c_from, h).wait_recv()
     for k in range(F):
         total = got[k, 0].astype(f32)
         for c in range(1, C):
@@ -430,12 +473,19 @@
     by_size(y, all_ended)
 
     def sent(block, carry):
-        for step in range(1, T):
-            s_copy(step, block, t).wait_send()
-        for step in range(1, C):
-            p_copy(step, block, chip).wait_send()
+        @pl.when(block != last_block(y))
+        def _():
+            for step in range(1, T):
+                s_copy(step, block, t).wait_send()
+            for step in range(1, C):
+                p_copy(step, block, chip).wait_send()
         return carry
     lax.fori_loop(0, F, sent, 0)
+    for h in range(H):
+        for step in range(1, T):
+            s_copy(step, last_block(y), t, h).wait_send()
+        for step in range(1, C):
+            p_copy(step, last_block(y), chip, h).wait_send()
 
 
 def solution(mesh):
@@ -451,26 +501,28 @@
             gt, ut = (lax.dynamic_slice_in_dim(v, lax.axis_index("tp") * columns, columns, 1) for v in (gate_taps, up_taps))
         margin = max(pool_spans)
         vmem = pl.BlockSpec(memory_space=pltpu.VMEM)
-        anywhere = pl.BlockSpec(memory_space=pl.ANY)
         dma = pltpu.SemaphoreType.DMA
         S, PR = plan.pool_owners(groups)
         PC = PR * Y
+        H = plan.halves(depth)
+        K = 2 + H
         V = pltpu.VMEM
         return pl.pallas_call(
             functools.partial(kernel, plan),
-            out_shape=jax.ShapeDtypeStruct((rows, width), bf16),
-            in_specs=[vmem, vmem, anywhere, vmem, vmem, anywhere, anywhere, anywhere, vmem, vmem, vmem],
+            out_shape=pltpu.VMEM((rows, width), bf16),
+            in_specs=[pl.BlockSpec(memory_space=pltpu.HBM)] * 11,
             out_specs=vmem,
             scratch_shapes=[
+                V((rows, width), bf16), V((1, width), f32), V((1, width), f32), V((1, width), f32), V(gt.shape, f32), V(ut.shape, f32), V((1, width), f32),
                 V((margin, width), bf16), V((groups, Z, gc // Z, gc), bf16), V((F, 2, depth, cols), bf16), V((F, cols, depth), bf16),
                 V((G, F, rows, depth), bf16), V((margin + rows, width), f32), V((rows, width), f32),
                 V((8 + G * rows, cols), f32), V((8 + G * rows, cols), f32), V((G, rows, cols), bf16),
                 V((F, T, C, rows, depth), bf16), V((F, max(T - 1, 1), C, rows, depth), bf16), V((F, C, rows, depth), bf16), V((F, C, rows, depth), bf16),
-                dma((4,)), dma((2,)), dma((3, max(Y - 1, 1))), dma((3, F)), dma((3, F)), dma((3, F)),
+                dma((7,)), dma((K + 1,)), dma((2,)), dma((K, max(Y - 1, 1))), dma((K, F)), dma((K, F)), dma((K, F)),
                 dma((max(Z - 1, 1),)), dma((Z,)), dma((max(PC - 1, 1),)), dma((PC,)), dma((max(S - 1, 1), PR)), dma((PR, S)), dma((max(C - 1, 1),)), dma((G,)),
-                dma((max(T - 1, 1), C)), dma((F, max(T - 1, 1))), dma((F, T)), dma((F, max(C - 1, 1))), dma((F, C)),
+                dma((max(T - 1, 1), C)), dma((F + H, max(T - 1, 1))), dma((F + H, T)), dma((F + H, max(C - 1, 1))), dma((F + H, C)),
             ],
-            compiler_params=pltpu.CompilerParams(has_side_effects=True, collective_id=0, vmem_limit_bytes=52 * 2**20),
+            compiler_params=pltpu.CompilerParams(has_side_effects=True, collective_id=0, vmem_limit_bytes=54 * 2**20),
             name="layer",
         )(tokens, gain_in[None], pool, gain_out[None], gain_ffn[None], gate_w, up_w, down_w, gt, ut, gain_last[None])
 

time: 172 us -> 165 us (0.959)
  local copies, waits for them, and re-layouts: 6.4 us -> 0.88 us
    unnamed x15 -> x1, local copies, waits for them, and re-layouts: 6.4 us -> 0.88 us
where the time goes in v3:
time: 165 us
  Pallas kernels  164 us (99%)
    pallas_call x1, Pallas kernels, shards(): pl.pallas_call(functools.partial(kernel, plan), out_shape=pltpu.VMEM((row...  164 us

profile of v3, /device:TPU:0, one launch (start us, length us, event | category | flops | bytes accessed | tf_op | source)
XLA Modules:
  0.0 165.2 jit_solution(16633024247457158185)
XLA Ops:
  0.0 164.3 %layer.1 = bf16[192,2048]{1,0:T(8,128)(2,1)S(1)} custom-call(bf16[192,2048]{1,0:T(8,128)(2,1)} %tokens_hbm.1, f32[1,2048]{1,0:T(1,128)} %bitcast.4, bf16[4,64,512]{2,1,0:T(8,128)(2,1)} %pool.1, f32[1,2048]{1,0:T(1,128)} %bitcast.5, f32[1,2048]{1,0:T(1,128)} %bitcast.6, bf16[256,2816]{1,0:T(8,128)(2,1)} %gate_w.1, bf16[256,2816]{1,0:T(8,128)(2,1)} %up_w.1, ...), custom_call_target="tpu_custom_call" | custom-call | tf_op jit(solution)/shard_map/layer/pallas_call | solution.py:510
  164.3 0.9 copy.13

commit v4 on v3

--- a/solution.py
+++ b/solution.py
@@ -234,11 +234,11 @@
     def flag(block, h):
         return block if h is None else F + h
 
-    def s_copy(step, block, t_from, h=None):
+    def s_copy(step, block, t_from, c, h=None):
         t_to = (t + step) % T
         return pltpu.make_async_remote_copy(
-            src_ref=partial.at[block, t_to, :, :, part(h)], dst_ref=swapped.at[block, step - 1, :, :, part(h)],
-            send_sem=s_ss.at[flag(block, h), step - 1], recv_sem=s_rs.at[flag(block, h), t_from],
+            src_ref=partial.at[block, t_to, c, :, part(h)], dst_ref=swapped.at[block, step - 1, c, :, part(h)],
+            send_sem=s_ss.at[flag(block, h), step - 1, c], recv_sem=s_rs.at[flag(block, h), t_from, c],
             device_id={"tp": t_to}, device_id_type=MESH)
 
     def p_copy(step, block, c_from, h=None):
@@ -325,12 +325,18 @@
     def times(lhs, rhs):
         return jnp.dot(lhs, rhs, preferred_element_type=f32)
 
+    def place_of(g):
+        return pl.multiple_of(8 + g // T * (8 + T * rows) + g % T * rows, 8)
+
+    def gate_up_group(origin, g):
+        x = x_all[g, origin]
+        at = pl.ds(place_of(g), rows)
+        acc_g[at, :] += times(x, w_gu[origin, 0])
+        acc_u[at, :] += times(x, w_gu[origin, 1])
+
     def gate_up(origin):
         def body(g, carry):
-            x = x_all[g, origin]
-            at = pl.ds(pl.multiple_of(8 + g * rows, 8), rows)
-            acc_g[at, :] += times(x, w_gu[origin, 0])
-            acc_u[at, :] += times(x, w_gu[origin, 1])
+            gate_up_group(origin, g)
             return carry
         lax.fori_loop(0, G, body, 0)
 
@@ -355,73 +361,85 @@
             chain(GU, k)
         gate_up(place(k)[1])
         return carry
-    lax.fori_loop(0, F, gate_up_step, 0)
+    lax.fori_loop(0, F - 1, gate_up_step, 0)
     chain_range(DNS, Y, jnp.minimum(ahead, F - 1))
+
+    @pl.when(F - 1 >= early)
+    def _():
+        chain(GU, F - 1)
 
     taps = gate_taps.shape[0]
     window = pl.ds(pl.multiple_of(t * plan.tiles * lanes + plan.first_tile(sub_of(y), t) * lanes, lanes), cols) if plan.joined else slice(None)
 
-    def convolve(acc, taps_ref, g, keep):
-        block = acc[pl.ds(pl.multiple_of(g * rows, 8), rows + 8), :]
+    def convolve(acc, taps_ref, g):
+        block = acc[pl.ds(pl.multiple_of(place_of(g) - 8, 8), rows + 8), :]
         total = taps_ref[taps - 1 : taps, window] * block[8:]
         for back in range(1, taps):
-            moved = pltpu.roll(block, back, 0)[8:]
-            total = total + taps_ref[taps - 1 - back : taps - back, window] * jnp.where(keep >= back, moved, 0.0)
+            total = total + taps_ref[taps - 1 - back : taps - back, window] * pltpu.roll(block, back, 0)[8:]
         return total
 
-    def activate(g, carry):
-        keep = (g % T) * rows + lax.broadcasted_iota(jnp.int32, (rows, cols), 0)
-        hidden[g] = (gelu(convolve(acc_g, gate_taps, g, keep)) * convolve(acc_u, up_taps, g, keep)).astype(bf16)
-        return carry
-
-    lax.fori_loop(0, G, activate, 0)
-
-    def down(block, h=None):
-        def body(i, carry):
-            step, c = i // C + 1, i % C
+    def activate(c):
+        def body(t_from, carry):
+            g = c * T + t_from
+            gate_up_group(place(F - 1)[1], g)
+            hidden[g] = (gelu(convolve(acc_g, gate_taps, g)) * convolve(acc_u, up_taps, g)).astype(bf16)
+            return carry
+        lax.fori_loop(0, T, body, 0)
+
+    def multiply(block, c, h):
+        for step in range(1, T):
             t_to = (t + step) % T
             product = jnp.dot(hidden[c * T + t_to], w_d[block, :, part(h)], preferred_element_type=f32)
             partial[block, t_to, c, :, part(h)] = product.astype(bf16)
-            return carry
-        lax.fori_loop(0, G - C, body, 0)
-        for step in range(1, T):
-            s_copy(step, block, t, h).start()
-        lax.fori_loop(G - C, G, body, 0)
-
-    def add_up(block, h=None):
+            s_copy(step, block, t, c, h).start()
+        product = jnp.dot(hidden[c * T + t], w_d[block, :, part(h)], preferred_element_type=f32)
+        partial[block, t, c, :, part(h)] = product.astype(bf16)
+
+    def add_up(block, c, h):
         for back in range(1, T):
-            s_copy(back, block, (t + back) % T, h).wait_recv()
-
-        def body(c, carry):
-            total = partial[block, t, c, :, part(h)].astype(f32)
-            for back in range(1, T):
-                total = total + swapped[block, T - 1 - back, c, :, part(h)].astype(f32)
-            summed[block, c, :, part(h)] = total.astype(bf16)
+            s_copy(back, block, (t + back) % T, c, h).wait_recv()
+        total = partial[block, t, c, :, part(h)].astype(f32)
+        for back in range(1, T):
+            total = total + swapped[block, T - 1 - back, c, :, part(h)].astype(f32)
+        summed[block, c, :, part(h)] = total.astype(bf16)
+
+        @pl.when(c != chip)
+        def _():
+            p_copy((c + C - chip) % C, block, chip, h).start()
+
+        @pl.when(c == chip)
+        def _():
+            got[block, chip, :, part(h)] = summed[block, chip, :, part(h)]
+
+    def down(block, h=None, before=None):
+        def body(i, carry):
+            if before is not None:
+                before((chip + 1 + i) % C)
+            multiply(block, (chip + 1 + i) % C, h)
+
+            @pl.when(i > 0)
+            def _():
+                add_up(block, (chip + i) % C, h)
             return carry
         lax.fori_loop(0, C, body, 0)
-        for step in range(1, C):
-            p_copy(step, block, chip, h).start()
-        got[block, chip, :, part(h)] = summed[block, chip, :, part(h)]
+        add_up(block, chip, h)
 
     def down_step(k, carry):
         @pl.when(k >= ahead)
         def _():
-            add_up(place(k - 1)[1])
             chain(DNS, k)
         down(place(k)[1])
-
-        @pl.when((k > 0) & (k < ahead))
-        def _():
-            add_up(place(k - 1)[1])
         return carry
-    lax.fori_loop(0, F - 1, down_step, 0)
+
     if F > 1:
-        add_up(place(F - 2)[1])
+        down(place(0)[1], before=activate)
+    else:
+        lax.fori_loop(0, C, lambda c, carry: (activate(c), carry)[1], 0)
+    lax.fori_loop(1, F - 1, down_step, 0)
     for h in range(H):
         if F > Y:
             chain((DNS[h],), F - 1)
         down(last_block(y), h)
-        add_up(last_block(y), h)
 
     def finish(block, carry):
         for step in range(1, C):
@@ -476,14 +494,16 @@
         @pl.when(block != last_block(y))
         def _():
             for step in range(1, T):
-                s_copy(step, block, t).wait_send()
+                for c in range(C):
+                    s_copy(step, block, t, c).wait_send()
             for step in range(1, C):
                 p_copy(step, block, chip).wait_send()
         return carry
     lax.fori_loop(0, F, sent, 0)
     for h in range(H):
         for step in range(1, T):
-            s_copy(step, last_block(y), t, h).wait_send()
+            for c in range(C):
+                s_copy(step, last_block(y), t, c, h).wait_send()
         for step in range(1, C):
             p_copy(step, last_block(y), chip, h).wait_send()
 
@@ -516,11 +536,11 @@
                 V((rows, width), bf16), V((1, width), f32), V((1, width), f32), V((1, width), f32), V(gt.shape, f32), V(ut.shape, f32), V((1, width), f32),
                 V((margin, width), bf16), V((groups, Z, gc // Z, gc), bf16), V((F, 2, depth, cols), bf16), V((F, cols, depth), bf16),
                 V((G, F, rows, depth), bf16), V((margin + rows, width), f32), V((rows, width), f32),
-                V((8 + G * rows, cols), f32), V((8 + G * rows, cols), f32), V((G, rows, cols), bf16),
+                V((C * (8 + T * rows), cols), f32), V((C * (8 + T * rows), cols), f32), V((G, rows, cols), bf16),
                 V((F, T, C, rows, depth), bf16), V((F, max(T - 1, 1), C, rows, depth), bf16), V((F, C, rows, depth), bf16), V((F, C, rows, depth), bf16),
                 dma((7,)), dma((K + 1,)), dma((2,)), dma((K, max(Y - 1, 1))), dma((K, F)), dma((K, F)), dma((K, F)),
                 dma((max(Z - 1, 1),)), dma((Z,)), dma((max(PC - 1, 1),)), dma((PC,)), dma((max(S - 1, 1), PR)), dma((PR, S)), dma((max(C - 1, 1),)), dma((G,)),
-                dma((max(T - 1, 1), C)), dma((F + H, max(T - 1, 1))), dma((F + H, T)), dma((F + H, max(C - 1, 1))), dma((F + H, C)),
+                dma((max(T - 1, 1), C)), dma((F + H, max(T - 1, 1), C)), dma((F + H, T, C)), dma((F + H, max(C - 1, 1))), dma((F + H, C)),
             ],
             compiler_params=pltpu.CompilerParams(has_side_effects=True, collective_id=0, vmem_limit_bytes=54 * 2**20),
             name="layer",

time: 165 us -> 167 us (1.012)
  Pallas kernels: 164 us -> 166 us
    pallas_call x1, Pallas kernels: 164 us -> 166 us  [shards(): pl.pallas_call(functools.partial(kernel, plan), out_shape=pltpu.VMEM((row...]
where the time goes in v4:
time: 167 us
  Pallas kernels  166 us (99%)
    pallas_call x1, Pallas kernels, shards(): pl.pallas_call(functools.partial(kernel, plan), out_shape=pltpu.VMEM((row...  166 us

profile of v4, /device:TPU:0, one launch (start us, length us, event | category | flops | bytes accessed | tf_op | source)
XLA Modules:
  0.0 167.3 jit_solution(1047189794288084498)
XLA Ops:
  0.0 166.4 %layer.1 = bf16[192,2048]{1,0:T(8,128)(2,1)S(1)} custom-call(bf16[192,2048]{1,0:T(8,128)(2,1)} %tokens_hbm.1, f32[1,2048]{1,0:T(1,128)} %bitcast.4, bf16[4,64,512]{2,1,0:T(8,128)(2,1)} %pool.1, f32[1,2048]{1,0:T(1,128)} %bitcast.5, f32[1,2048]{1,0:T(1,128)} %bitcast.6, bf16[256,2816]{1,0:T(8,128)(2,1)} %gate_w.1, bf16[256,2816]{1,0:T(8,128)(2,1)} %up_w.1, ...), custom_call_target="tpu_custom_call" | custom-call | tf_op jit(solution)/shard_map/layer/pallas_call | solution.py:530
  166.4 0.9 copy.13

commit v5 on v4

--- a/solution.py
+++ b/solution.py
@@ -231,20 +231,19 @@
             src_ref=x_all.at[g], dst_ref=x_all.at[g], send_sem=f_ss.at[step - 1, c],
             recv_sem=x_rs.at[g], device_id={"tp": (t + step) % T}, device_id_type=MESH)
 
-    def flag(block, h):
-        return block if h is None else F + h
-
-    def s_copy(step, block, t_from, c, h=None):
+    def s_copy(step, turn, block, t_from, c, h=None):
         t_to = (t + step) % T
-        return pltpu.make_async_remote_copy(
-            src_ref=partial.at[block, t_to, c, :, part(h)], dst_ref=swapped.at[block, step - 1, c, :, part(h)],
-            send_sem=s_ss.at[flag(block, h), step - 1, c], recv_sem=s_rs.at[flag(block, h), t_from, c],
+        window = (slice(None) if c is None else c, slice(None), part(h))
+        at = 0 if c is None else c
+        return pltpu.make_async_remote_copy(
+            src_ref=partial.at[(block, t_to) + window], dst_ref=swapped.at[(block, step - 1) + window],
+            send_sem=s_ss.at[turn % 2, step - 1, at], recv_sem=s_rs.at[turn % 2, t_from, at],
             device_id={"tp": t_to}, device_id_type=MESH)
 
     def p_copy(step, block, c_from, h=None):
         return pltpu.make_async_remote_copy(
             src_ref=summed.at[block, (chip + step) % C, :, part(h)], dst_ref=got.at[block, c_from, :, part(h)],
-            send_sem=p_ss.at[flag(block, h), step - 1], recv_sem=p_rs.at[flag(block, h), c_from],
+            send_sem=p_ss.at[block, step - 1], recv_sem=p_rs.at[block, c_from],
             device_id=peer(step), device_id_type=MESH)
 
     def last_block(y_of):
@@ -362,7 +361,7 @@
         gate_up(place(k)[1])
         return carry
     lax.fori_loop(0, F - 1, gate_up_step, 0)
-    chain_range(DNS, Y, jnp.minimum(ahead, F - 1))
+    chain_range(DNS, Y, ahead)
 
     @pl.when(F - 1 >= early)
     def _():
@@ -379,25 +378,34 @@
         return total
 
     def activate(c):
-        def body(t_from, carry):
+        def last_step(t_from, carry):
+            gate_up_group(place(F - 1)[1], c * T + t_from)
+            return carry
+
+        def hide(t_from, carry):
             g = c * T + t_from
-            gate_up_group(place(F - 1)[1], g)
-            hidden[g] = (gelu(convolve(acc_g, gate_taps, g)) * convolve(acc_u, up_taps, g)).astype(bf16)
+            hidden[t_from, c] = (gelu(convolve(acc_g, gate_taps, g)) * convolve(acc_u, up_taps, g)).astype(bf16)
+            return carry
+        lax.fori_loop(0, T, last_step, 0)
+        lax.fori_loop(0, T, hide, 0)
+
+    def multiply(block, c):
+        def body(i, carry):
+            t_to = (t + 1 + i) % T
+            partial[block, t_to, c] = jnp.dot(hidden[t_to, c], w_d[block], preferred_element_type=f32).astype(bf16)
+
+            @pl.when(i < T - 1)
+            def _():
+                s_copy(i + 1, 0, block, t, c).start()
             return carry
         lax.fori_loop(0, T, body, 0)
 
-    def multiply(block, c, h):
-        for step in range(1, T):
-            t_to = (t + step) % T
-            product = jnp.dot(hidden[c * T + t_to], w_d[block, :, part(h)], preferred_element_type=f32)
-            partial[block, t_to, c, :, part(h)] = product.astype(bf16)
-            s_copy(step, block, t, c, h).start()
-        product = jnp.dot(hidden[c * T + t], w_d[block, :, part(h)], preferred_element_type=f32)
-        partial[block, t, c, :, part(h)] = product.astype(bf16)
+    def wait_swap(turn, block, c, h):
+        for back in range(1, T):
+            s_copy(back, turn, block, (t + back) % T, c, h).wait_recv()
+            s_copy(back, turn, block, t, c, h).wait_send()
 
     def add_up(block, c, h):
-        for back in range(1, T):
-            s_copy(back, block, (t + back) % T, c, h).wait_recv()
         total = partial[block, t, c, :, part(h)].astype(f32)
         for back in range(1, T):
             total = total + swapped[block, T - 1 - back, c, :, part(h)].astype(f32)
@@ -411,54 +419,48 @@
         def _():
             got[block, chip, :, part(h)] = summed[block, chip, :, part(h)]
 
-    def down(block, h=None, before=None):
+    lag = min(2, C)
+
+    def down_first(block):
         def body(i, carry):
-            if before is not None:
-                before((chip + 1 + i) % C)
-            multiply(block, (chip + 1 + i) % C, h)
-
-            @pl.when(i > 0)
+            activate((chip + 1 + i) % C)
+            multiply(block, (chip + 1 + i) % C)
+
+            @pl.when(i >= lag)
             def _():
-                add_up(block, (chip + i) % C, h)
+                wait_swap(0, block, (chip + 1 + i - lag) % C, None)
+                add_up(block, (chip + 1 + i - lag) % C, None)
             return carry
         lax.fori_loop(0, C, body, 0)
-        add_up(block, chip, h)
+        for i in range(C - lag, C):
+            wait_swap(0, block, (chip + 1 + i) % C, None)
+            add_up(block, (chip + 1 + i) % C, None)
+
+    def down_half(turn, block, h):
+        def body(i, carry):
+            t_to = (t + 1 + i) % T
+            product = jnp.dot(hidden[t_to].reshape(C * rows, cols), w_d[block, :, part(h)], preferred_element_type=f32)
+            partial[block, t_to, :, :, part(h)] = product.astype(bf16).reshape(C, rows, half)
+
+            @pl.when(i < T - 1)
+            def _():
+                s_copy(i + 1, turn, block, t, None, h).start()
+            return carry
+        lax.fori_loop(0, T, body, 0)
+        wait_swap(turn, block, None, h)
+        for i in range(C):
+            add_up(block, (chip + 1 + i) % C, h)
 
     def down_step(k, carry):
-        @pl.when(k >= ahead)
-        def _():
-            chain(DNS, k)
-        down(place(k)[1])
+        for h in range(H):
+            @pl.when(k >= ahead)
+            def _():
+                chain((DNS[h],), k)
+            down_half(1 + (k - 1) * H + h, place(k)[1], h)
         return carry
 
-    if F > 1:
-        down(place(0)[1], before=activate)
-    else:
-        lax.fori_loop(0, C, lambda c, carry: (activate(c), carry)[1], 0)
-    lax.fori_loop(1, F - 1, down_step, 0)
-    for h in range(H):
-        if F > Y:
-            chain((DNS[h],), F - 1)
-        down(last_block(y), h)
-
-    def finish(block, carry):
-        for step in range(1, C):
-            @pl.when(block != last_block((chip + step) % C % Y))
-            def _():
-                p_copy(step, block, (chip + step) % C).wait_recv()
-        return carry
-
-    lax.fori_loop(0, F, finish, 0)
-    for step in range(1, C):
-        for h in range(H):
-            c_from = (chip + step) % C
-            p_copy(step, last_block(c_from % Y), c_from, h).wait_recv()
-    for k in range(F):
-        total = got[k, 0].astype(f32)
-        for c in range(1, C):
-            total = total + got[k, c].astype(f32)
-        normed[pl.ds(0, rows), k * depth : (k + 1) * depth] = total
-    out[...] = (after[...] + rms_scale(normed[pl.ds(0, rows), :], gain_last[...])).astype(bf16)
+    down_first(place(0)[1])
+    lax.fori_loop(1, F, down_step, 0)
 
     halo_copy().wait_send()
     for step in range(1, Z):
@@ -493,19 +495,25 @@
     def sent(block, carry):
         @pl.when(block != last_block(y))
         def _():
-            for step in range(1, T):
-                for c in range(C):
-                    s_copy(step, block, t, c).wait_send()
             for step in range(1, C):
                 p_copy(step, block, chip).wait_send()
         return carry
     lax.fori_loop(0, F, sent, 0)
-    for h in range(H):
-        for step in range(1, T):
-            for c in range(C):
-                s_copy(step, last_block(y), t, c, h).wait_send()
+    def finish(block, carry):
         for step in range(1, C):
-            p_copy(step, last_block(y), chip, h).wait_send()
+            p_copy(step, block, (chip + step) % C).wait_recv()
+        return carry
+
+    lax.fori_loop(0, F, finish, 0)
+    for k in range(F):
+        total = got[k, 0].astype(f32)
+        for c in range(1, C):
+            total = total + got[k, c].astype(f32)
+        normed[pl.ds(0, rows), k * depth : (k + 1) * depth] = total
+    out[...] = (after[...] + rms_scale(normed[pl.ds(0, rows), :], gain_last[...])).astype(bf16)
+
+    for step in range(1, C):
+        p_copy(step, last_block(y), chip).wait_send()
 
 
 def solution(mesh):
@@ -536,11 +544,11 @@
                 V((rows, width), bf16), V((1, width), f32), V((1, width), f32), V((1, width), f32), V(gt.shape, f32), V(ut.shape, f32), V((1, width), f32),
                 V((margin, width), bf16), V((groups, Z, gc // Z, gc), bf16), V((F, 2, depth, cols), bf16), V((F, cols, depth), bf16),
                 V((G, F, rows, depth), bf16), V((margin + rows, width), f32), V((rows, width), f32),
-                V((C * (8 + T * rows), cols), f32), V((C * (8 + T * rows), cols), f32), V((G, rows, cols), bf16),
+                V((C * (8 + T * rows), cols), f32), V((C * (8 + T * rows), cols), f32), V((T, C, rows, cols), bf16),
                 V((F, T, C, rows, depth), bf16), V((F, max(T - 1, 1), C, rows, depth), bf16), V((F, C, rows, depth), bf16), V((F, C, rows, depth), bf16),
                 dma((7,)), dma((K + 1,)), dma((2,)), dma((K, max(Y - 1, 1))), dma((K, F)), dma((K, F)), dma((K, F)),
                 dma((max(Z - 1, 1),)), dma((Z,)), dma((max(PC - 1, 1),)), dma((PC,)), dma((max(S - 1, 1), PR)), dma((PR, S)), dma((max(C - 1, 1),)), dma((G,)),
-                dma((max(T - 1, 1), C)), dma((F + H, max(T - 1, 1), C)), dma((F + H, T, C)), dma((F + H, max(C - 1, 1))), dma((F + H, C)),
+                dma((max(T - 1, 1), C)), dma((2, max(T - 1, 1), C)), dma((2, T, C)), dma((F, max(C - 1, 1))), dma((F, C)),
             ],
             compiler_params=pltpu.CompilerParams(has_side_effects=True, collective_id=0, vmem_limit_bytes=54 * 2**20),
             name="layer",

time: 167 us -> 161 us (0.964)
  Pallas kernels: 166 us -> 160 us
    pallas_call x1, Pallas kernels: 166 us -> 160 us  [shards(): pl.pallas_call(functools.partial(kernel, plan), out_shape=pltpu.VMEM((row...]
where the time goes in v5:
time: 161 us
  Pallas kernels  160 us (99%)
    pallas_call x1, Pallas kernels, shards(): pl.pallas_call(functools.partial(kernel, plan), out_shape=pltpu.VMEM((row...  160 us

profile of v5, /device:TPU:0, one launch (start us, length us, event | category | flops | bytes accessed | tf_op | source)
XLA Modules:
  0.0 161.3 jit_solution(2983750906243790502)
XLA Ops:
  0.0 160.4 %layer.1 = bf16[192,2048]{1,0:T(8,128)(2,1)S(1)} custom-call(bf16[192,2048]{1,0:T(8,128)(2,1)} %tokens_hbm.1, f32[1,2048]{1,0:T(1,128)} %bitcast.4, bf16[4,64,512]{2,1,0:T(8,128)(2,1)} %pool.1, f32[1,2048]{1,0:T(1,128)} %bitcast.5, f32[1,2048]{1,0:T(1,128)} %bitcast.6, bf16[256,2816]{1,0:T(8,128)(2,1)} %gate_w.1, bf16[256,2816]{1,0:T(8,128)(2,1)} %up_w.1, ...), custom_call_target="tpu_custom_call" | custom-call | tf_op jit(solution)/shard_map/layer/pallas_call | solution.py:538
  160.4 0.9 copy.13

commit v6 on v5

--- a/solution.py
+++ b/solution.py
@@ -167,7 +167,7 @@
     def chain_copy(kind, origin, dz, size):
         block = slot(kind, origin, size)
         return pltpu.make_async_remote_copy(
-            src_ref=block, dst_ref=block, send_sem=(up_ss if dz > 0 else dn_ss).at[kind, origin],
+            src_ref=block, dst_ref=block, send_sem=(up_ss if dz > 0 else dn_ss).at[kind],
             recv_sem=piece_rs.at[kind, origin], device_id={"fs": (z + dz) * Y + y}, device_id_type=MESH)
 
     def pass_on(kind, origin, z0, size):
@@ -234,20 +234,17 @@
     def s_copy(step, turn, block, t_from, c, h=None):
         t_to = (t + step) % T
         window = (slice(None) if c is None else c, slice(None), part(h))
-        at = 0 if c is None else c
+        at = turn % 2 * C if c is None else c
         return pltpu.make_async_remote_copy(
             src_ref=partial.at[(block, t_to) + window], dst_ref=swapped.at[(block, step - 1) + window],
-            send_sem=s_ss.at[turn % 2, step - 1, at], recv_sem=s_rs.at[turn % 2, t_from, at],
+            send_sem=s_ss.at[step - 1, at], recv_sem=s_rs.at[t_from, at],
             device_id={"tp": t_to}, device_id_type=MESH)
 
     def p_copy(step, block, c_from, h=None):
         return pltpu.make_async_remote_copy(
             src_ref=summed.at[block, (chip + step) % C, :, part(h)], dst_ref=got.at[block, c_from, :, part(h)],
-            send_sem=p_ss.at[block, step - 1], recv_sem=p_rs.at[block, c_from],
+            send_sem=p_ss.at[step - 1], recv_sem=p_rs.at[block, c_from],
             device_id=peer(step), device_id_type=MESH)
-
-    def last_block(y_of):
-        return place(F - 1)[0] * Y + (y_of + (F - 1) % Y) % Y
 
     staged = [
         pltpu.make_async_copy(source_ref, held, in_sem.at[k]) for k, (source_ref, held) in enumerate((
@@ -420,6 +417,8 @@
             got[block, chip, :, part(h)] = summed[block, chip, :, part(h)]
 
     lag = min(2, C)
+    spread = [(dr, dy) for dr in range(R) for dy in range(Y)] if plan.joined else [(0, 0)]
+    far_first = sorted(spread, key=lambda d: -((d[0] > 0) + (d[1] > 0)))
 
     def down_first(block):
         def body(i, carry):
@@ -448,8 +447,8 @@
             return carry
         lax.fori_loop(0, T, body, 0)
         wait_swap(turn, block, None, h)
-        for i in range(C):
-            add_up(block, (chip + 1 + i) % C, h)
+        for dr, dy in far_first:
+            add_up(block, (r + dr) % R * Y + (y + dy) % Y if plan.joined else 0, h)
 
     def down_step(k, carry):
         for h in range(H):
@@ -478,42 +477,41 @@
     for step in range(1, Y):
         by_size((y + step) % Y, lambda size: [y_copy(kind, step, size).wait_send() for kind in kinds])
 
+    def every(kind, first, count, size):
+        if kind in DNS:
+            return w_d.at[pl.ds(first, count), pl.ds(0, size), part(kind - DN)]
+        return w_gu.at[pl.ds(first, count), kind - GA, :, pl.ds(0, size)]
+
     def all_ended(size):
-        for kind in kinds:
-            def ended(origin, carry):
-                @pl.when((origin // Y <= z) & (z + 1 < Z))
-                def _():
-                    chain_copy(kind, origin, 1, size).wait_send()
-
-                @pl.when((origin // Y >= z) & (z > 0))
-                def _():
-                    chain_copy(kind, origin, -1, size).wait_send()
-                return carry
-            lax.fori_loop(0, F, ended, 0)
+        for layer in range(Z):
+            @pl.when(z == layer)
+            def _():
+                for kind in kinds:
+                    for first, count, dz, sem in ((0, layer * Y + Y, 1, up_ss), (layer * Y, F - layer * Y, -1, dn_ss)):
+                        if 0 <= layer + dz < Z:
+                            block = every(kind, first, count, size)
+                            pltpu.make_async_remote_copy(
+                                src_ref=block, dst_ref=block, send_sem=sem.at[kind], recv_sem=piece_rs.at[kind, 0],
+                                device_id={"fs": (z + dz) * Y + y}, device_id_type=MESH).wait_send()
     by_size(y, all_ended)
 
-    def sent(block, carry):
-        @pl.when(block != last_block(y))
-        def _():
-            for step in range(1, C):
-                p_copy(step, block, chip).wait_send()
-        return carry
-    lax.fori_loop(0, F, sent, 0)
-    def finish(block, carry):
+    def finish(k, carry):
+        block = place(k)[1]
         for step in range(1, C):
             p_copy(step, block, (chip + step) % C).wait_recv()
+        total = got[block, 0].astype(f32)
+        for c in range(1, C):
+            total = total + got[block, c].astype(f32)
+        normed[pl.ds(0, rows), pl.ds(pl.multiple_of(block * depth, depth), depth)] = total
         return carry
 
     lax.fori_loop(0, F, finish, 0)
-    for k in range(F):
-        total = got[k, 0].astype(f32)
-        for c in range(1, C):
-            total = total + got[k, c].astype(f32)
-        normed[pl.ds(0, rows), k * depth : (k + 1) * depth] = total
     out[...] = (after[...] + rms_scale(normed[pl.ds(0, rows), :], gain_last[...])).astype(bf16)
 
     for step in range(1, C):
-        p_copy(step, last_block(y), chip).wait_send()
+        pltpu.make_async_remote_copy(
+            src_ref=summed.at[:, (chip + step) % C], dst_ref=got.at[:, chip], send_sem=p_ss.at[step - 1],
+            recv_sem=p_rs.at[0, chip], device_id=peer(step), device_id_type=MESH).wait_send()
 
 
 def solution(mesh):
@@ -546,9 +544,9 @@
                 V((G, F, rows, depth), bf16), V((margin + rows, width), f32), V((rows, width), f32),
                 V((C * (8 + T * rows), cols), f32), V((C * (8 + T * rows), cols), f32), V((T, C, rows, cols), bf16),
                 V((F, T, C, rows, depth), bf16), V((F, max(T - 1, 1), C, rows, depth), bf16), V((F, C, rows, depth), bf16), V((F, C, rows, depth), bf16),
-                dma((7,)), dma((K + 1,)), dma((2,)), dma((K, max(Y - 1, 1))), dma((K, F)), dma((K, F)), dma((K, F)),
+                dma((7,)), dma((K + 1,)), dma((2,)), dma((K, max(Y - 1, 1))), dma((K,)), dma((K,)), dma((K, F)),
                 dma((max(Z - 1, 1),)), dma((Z,)), dma((max(PC - 1, 1),)), dma((PC,)), dma((max(S - 1, 1), PR)), dma((PR, S)), dma((max(C - 1, 1),)), dma((G,)),
-                dma((max(T - 1, 1), C)), dma((2, max(T - 1, 1), C)), dma((2, T, C)), dma((F, max(C - 1, 1))), dma((F, C)),
+                dma((max(T - 1, 1), C)), dma((max(T - 1, 1), C + 1)), dma((T, C + 1)), dma((max(C - 1, 1),)), dma((F, C)),
             ],
             compiler_params=pltpu.CompilerParams(has_side_effects=True, collective_id=0, vmem_limit_bytes=54 * 2**20),
             name="layer",

time: 161 us -> 161 us (level)
  no operation moved by 1% of the time
where the time goes in v6:
time: 161 us; the launch traced here: 160 us
  Pallas kernels  160 us (99%)
    pallas_call x1, Pallas kernels, shards(): pl.pallas_call(functools.partial(kernel, plan), out_shape=pltpu.VMEM((row...  160 us

profile of v6, /device:TPU:0, one launch (start us, length us, event | category | flops | bytes accessed | tf_op | source)
XLA Modules:
  0.0 160.4 jit_solution(9784549382794888585)
XLA Ops:
  0.0 159.5 %layer.1 = bf16[192,2048]{1,0:T(8,128)(2,1)S(1)} custom-call(bf16[192,2048]{1,0:T(8,128)(2,1)} %tokens_hbm.1, f32[1,2048]{1,0:T(1,128)} %bitcast.4, bf16[4,64,512]{2,1,0:T(8,128)(2,1)} %pool.1, f32[1,2048]{1,0:T(1,128)} %bitcast.5, f32[1,2048]{1,0:T(1,128)} %bitcast.6, bf16[256,2816]{1,0:T(8,128)(2,1)} %gate_w.1, bf16[256,2816]{1,0:T(8,128)(2,1)} %up_w.1, ...), custom_call_target="tpu_custom_call" | custom-call | tf_op jit(solution)/shard_map/layer/pallas_call | solution.py:536
  159.5 0.9 copy.13

commit v7 on v6

--- a/solution.py
+++ b/solution.py
@@ -450,11 +450,13 @@
         for dr, dy in far_first:
             add_up(block, (r + dr) % R * Y + (y + dy) % Y if plan.joined else 0, h)
 
+    lead = jnp.where(side > 0, jnp.minimum(4, ahead - 1), 0)
+
     def down_step(k, carry):
         for h in range(H):
-            @pl.when(k >= ahead)
+            @pl.when((k + lead >= ahead) & (k + lead < F))
             def _():
-                chain((DNS[h],), k)
+                chain((DNS[h],), k + lead)
             down_half(1 + (k - 1) * H + h, place(k)[1], h)
         return carry
 
@@ -503,10 +505,10 @@
         for c in range(1, C):
             total = total + got[block, c].astype(f32)
         normed[pl.ds(0, rows), pl.ds(pl.multiple_of(block * depth, depth), depth)] = total
-        return carry
-
-    lax.fori_loop(0, F, finish, 0)
-    out[...] = (after[...] + rms_scale(normed[pl.ds(0, rows), :], gain_last[...])).astype(bf16)
+        return carry + jnp.sum(total * total, axis=-1, keepdims=True)
+
+    squares = lax.fori_loop(0, F, finish, jnp.zeros((rows, 1), f32))
+    out[...] = (after[...] + normed[pl.ds(0, rows), :] * lax.rsqrt(squares / width + rms_eps) * gain_last[...]).astype(bf16)
 
     for step in range(1, C):
         pltpu.make_async_remote_copy(

time: 161 us -> 160 us (level)
  no operation moved by 1% of the time
where the time goes in v7:
time: 160 us
  Pallas kernels  159 us (99%)
    pallas_call x1, Pallas kernels, shards(): pl.pallas_call(functools.partial(kernel, plan), out_shape=pltpu.VMEM((row...  159 us

profile of v7, /device:TPU:0, one launch (start us, length us, event | category | flops | bytes accessed | tf_op | source)
XLA Modules:
  0.0 160.1 jit_solution(18309033912883364037)
XLA Ops:
  0.0 159.2 %layer.1 = bf16[192,2048]{1,0:T(8,128)(2,1)S(1)} custom-call(bf16[192,2048]{1,0:T(8,128)(2,1)} %tokens_hbm.1, f32[1,2048]{1,0:T(1,128)} %bitcast.4, bf16[4,64,512]{2,1,0:T(8,128)(2,1)} %pool.1, f32[1,2048]{1,0:T(1,128)} %bitcast.5, f32[1,2048]{1,0:T(1,128)} %bitcast.6, bf16[256,2816]{1,0:T(8,128)(2,1)} %gate_w.1, bf16[256,2816]{1,0:T(8,128)(2,1)} %up_w.1, ...), custom_call_target="tpu_custom_call" | custom-call | tf_op jit(solution)/shard_map/layer/pallas_call | solution.py:538
  159.2 0.9 copy.13
